TPU v7x, 128 devices: a whole 4x4x4 slice. The times are simulated.
128 devices in a mesh: ep: 64 (over z, y, x), tp: 2 (over core).
Axes of the slice: x: 4, y: 4, z: 4, core: 2. Of those that a mesh axis runs over, the one named last changes fastest.
Arguments:
- tokens: bfloat16 [1536, 2048], P('ep'), may hold values from -6 to 6
- attn_gain: float32 [2048], replicated, may hold values from 0.1 to 1.9
- w_query: bfloat16 [2048, 1024], P(None, 'tp'), may hold values from -0.125 to 0.125
- w_key: bfloat16 [2048, 1024], P(None, 'tp'), may hold values from -0.125 to 0.125
- w_value: bfloat16 [2048, 1024], P(None, 'tp'), may hold values from -0.125 to 0.125
- w_zgate: bfloat16 [2048, 1024], P(None, 'tp'), may hold values from -0.125 to 0.125
- w_decay: bfloat16 [2048, 8], P(None, 'tp'), may hold values from -0.125 to 0.125
- w_beta: bfloat16 [2048, 8], P(None, 'tp'), may hold values from -0.125 to 0.125
- decay_rate: float32 [8], P('tp'), may hold values from 0.05 to 2
- decay_bias: float32 [8], P('tp'), may hold values from -3 to 3
- state: float32 [1536, 8, 128, 128], P('ep', 'tp'), may hold values from -2 to 2
- out_gain: float32 [128], replicated, may hold values from 0.1 to 1.9
- w_out: bfloat16 [1024, 2048], P('tp'), may hold values from -0.1875 to 0.1875
- ffn_gain: float32 [2048], replicated, may hold values from 0.1 to 1.9
- expert_gate: bfloat16 [64, 2048, 512], P('ep', None, 'tp'), may hold values from -0.125 to 0.125
- expert_up: bfloat16 [64, 2048, 512], P('ep', None, 'tp'), may hold values from -0.125 to 0.125
- expert_down: bfloat16 [64, 512, 2048], P('ep', 'tp'), may hold values from -0.25 to 0.25
- routes: int32 [1536, 2], P('ep'), may hold values from 0 to 63, all different within a row; in each aligned block of 24 rows (0 to 23, 24 to 47, ...) at most 2 rows name the same one
- route_weight: float32 [1536, 2], P('ep'), may hold values from 0.2 to 1
Outputs:
- layer_out: bfloat16 [1536, 2048], P('ep', 'tp')
- new_state: float32 [1536, 8, 128, 128], P('ep', 'tp')
Inputs may be any that keep to these rules, and one draw needn't show every extreme that they name: `routes`: the 2 entries of a row differ. Among the rows of one index of ep (aligned blocks of 24 rows) no expert is named more than 2 times, a bound that some block reaches.
All inputs are finite; a program needn't handle non-finite values.
Results may differ from a plain program's by a relative error of at most 0.014.
Values may be sent and summed in bfloat16 or wider, within the bound.
A program may use at most 128 MiB of HBM per device.

v0:
```python
import jax
import jax.numpy as jnp
from jax import lax
from jax.sharding import PartitionSpec as P

EPS = 1e-06


def copy_for_each(value, axis):
    peers = lax.axis_size(axis)
    return lax.all_to_all(
        jnp.broadcast_to(value[None], (peers, *value.shape)), axis, 0, 0, tiled=True
    )


def taken_together(value, axis):
    return copy_for_each(value, axis).astype(jnp.float32).sum(axis=0)


def split_up(value, dim, peers):
    dims = value.shape
    tiles = value.reshape(*dims[:dim], peers, dims[dim] // peers, *dims[dim + 1 :])
    return jnp.moveaxis(tiles, dim, 0)


def sum_at_owner(value, axis, dim):
    tiles = split_up(value, dim, lax.axis_size(axis))
    arrived = lax.all_to_all(tiles, axis, split_axis=0, concat_axis=0, tiled=True)
    return arrived.astype(jnp.float32).sum(axis=0)


def rms_scale(rows, gain):
    return rows * lax.rsqrt(jnp.mean(rows * rows, axis=-1, keepdims=True) + EPS) * gain


def unit_rows(rows):
    return rows * lax.rsqrt(jnp.sum(rows * rows, axis=-1, keepdims=True) + EPS)


def per_device(
    tokens,
    attn_gain,
    w_query,
    w_key,
    w_value,
    w_zgate,
    w_decay,
    w_beta,
    decay_rate,
    decay_bias,
    state,
    out_gain,
    w_out,
    ffn_gain,
    expert_gate,
    expert_up,
    expert_down,
    routes,
    route_weight,
):
    seqs, width = tokens.shape
    heads = state.shape[1]
    head_dim = state.shape[2]
    top = routes.shape[1]
    resid_in = tokens.astype(jnp.float32)
    normed = rms_scale(resid_in, attn_gain).astype(jnp.bfloat16)

    def project(weight):
        return jnp.dot(normed, weight, preferred_element_type=jnp.float32).astype(jnp.bfloat16)

    def heads_of(raw):
        return raw.reshape(seqs, heads, head_dim).astype(jnp.float32)

    query = unit_rows(jax.nn.silu(heads_of(project(w_query)))) * head_dim ** (-0.5)
    key = unit_rows(jax.nn.silu(heads_of(project(w_key))))
    value = jax.nn.silu(heads_of(project(w_value)))
    zmul = jax.nn.silu(heads_of(project(w_zgate)))
    fade = jnp.exp(-decay_rate * jax.nn.softplus(project(w_decay).astype(jnp.float32) + decay_bias))
    beta = jax.nn.sigmoid(project(w_beta).astype(jnp.float32))
    predicted = jnp.einsum("shkv,shk->shv", state, key)
    written = beta[..., None] * (value - fade[..., None] * predicted)
    new_state = fade[..., None, None] * state + key[..., :, None] * written[..., None, :]
    read = jnp.einsum("shkv,shk->shv", new_state, query)
    heads_out = (
        (rms_scale(read, out_gain) * zmul).astype(jnp.bfloat16).reshape(seqs, heads * head_dim)
    )
    partial_value = jnp.dot(heads_out, w_out, preferred_element_type=jnp.float32)
    mixed = taken_together(partial_value.astype(jnp.bfloat16), "tp").astype(jnp.float32)
    resid = resid_in + mixed
    moe_in = rms_scale(resid, ffn_gain).astype(jnp.bfloat16)
    experts = lax.axis_size("ep")
    cap = max(2, 2 * seqs * top // experts)
    flat_routes = routes.reshape(-1)
    onehot = (flat_routes[:, None] == jnp.arange(experts, dtype=jnp.int32)[None, :]).astype(
        jnp.int32
    )
    before = jnp.cumsum(onehot, axis=0) - onehot
    slot = jnp.sum(before * onehot, axis=1)
    place = flat_routes * cap + slot
    pick = (place[:, None] == jnp.arange(experts * cap, dtype=jnp.int32)[None, :]).astype(
        jnp.bfloat16
    )
    columns = width // lax.axis_size("tp")
    spread = jnp.repeat(moe_in, top, axis=0)
    outgoing = jnp.dot(pick.T, spread, preferred_element_type=jnp.float32).astype(jnp.bfloat16)
    outgoing = outgoing.reshape(experts, 1, cap, width)
    arrived = lax.all_to_all(outgoing, "ep", split_axis=0, concat_axis=1, tiled=True)
    flat_rows = arrived.reshape(-1, arrived.shape[-1])
    gate = jnp.dot(flat_rows, expert_gate[0], preferred_element_type=jnp.float32)
    up = jnp.dot(flat_rows, expert_up[0], preferred_element_type=jnp.float32)
    hidden = (jax.nn.silu(gate) * up).astype(jnp.bfloat16)
    term = jnp.dot(hidden, expert_down[0], preferred_element_type=jnp.float32)
    terms = term.reshape(arrived.shape[:-1] + (term.shape[-1],))
    summed = sum_at_owner(terms.astype(jnp.bfloat16), "tp", 3).astype(jnp.bfloat16)
    returned = lax.all_to_all(summed, "ep", split_axis=1, concat_axis=0, tiled=True)
    returned = returned.reshape(experts * cap, columns)
    per_route = jnp.dot(pick, returned, preferred_element_type=jnp.float32).reshape(
        seqs, top, columns
    )
    combined = jnp.sum(per_route * route_weight[..., None], axis=1)
    own_resid = lax.dynamic_slice_in_dim(resid, lax.axis_index("tp") * columns, columns, 1)
    layer_out = (own_resid + combined).astype(jnp.bfloat16)
    return (layer_out, new_state)


def solution(mesh):
    in_specs = (
        P("ep", None),
        P(),
        P(None, "tp"),
        P(None, "tp"),
        P(None, "tp"),
        P(None, "tp"),
        P(None, "tp"),
        P(None, "tp"),
        P("tp"),
        P("tp"),
        P("ep", "tp", None, None),
        P(),
        P("tp", None),
        P(),
        P("ep", None, "tp"),
        P("ep", None, "tp"),
        P("ep", "tp", None),
        P("ep", None),
        P("ep", None),
    )
    out_specs = (P("ep", "tp"), P("ep", "tp", None, None))
    return jax.shard_map(
        per_device, mesh=mesh, in_specs=in_specs, out_specs=out_specs, check_vma=False
    )
```

profile of v0, /device:TPU:1, one launch (start us, length us, event | category | flops | bytes accessed | tf_op | source)
XLA Modules:
  0.0 79.3 jit_solution(15999648723681051084)
XLA Ops:
  0.7 1.2 %fusion.17 = f32[24]{0:T(128)S(1)} fusion(bf16[24,2048]{1,0:T(8,128)(2,1)} %param.19), kind=kLoop, calls=%fused_computation.34 | loop fusion | flops 147432 | bytes 98400 | tf_op jit(solution)/shard_map/reduce_sum | solution.py:33
  1.9 2.1 %fusion.5 = f32[24,512]{1,0:T(8,128)S(1)} fusion(bf16[2048,512]{1,0:T(8,128)(2,1)} %param.22, bf16[24,2048]{1,0:T(8,128)(2,1)} %param.19, f32[2048]{0:T(1024)} %param.20, f32[24]{0:T(128)S(1)} %add_rsqrt_fusion.4), kind=kOutput, calls=%fused_computation.15 | convolution fusion | flops 50552832 | bytes 2252896 | tf_op jit(solution)/shard_map/dot_general | solution.py:69
  4.0 0.1 multiply_reduce_fusion.3
  4.3 0.2 fusion.33
  4.6 2.0 %fusion.4 = f32[24,512]{1,0:T(8,128)S(1)} fusion(bf16[2048,512]{1,0:T(8,128)(2,1)} %param.23, bf16[24,2048]{1,0:T(8,128)(2,1)S(1)} %copy-done.2, f32[2048]{0:T(1024)S(1)} %copy-done.5, f32[24]{0:T(128)S(1)} %add_rsqrt_fusion.4), kind=kOutput, calls=%fused_computation.13 | convolution fusion | flops 50552832 | bytes 2252896 | tf_op jit(solution)/shard_map/dot_general | solution.py:69
  6.7 0.2 fusion.12
  7.0 3.9 %fusion.40 = f32[24,4,1,128]{3,2,1,0:T(1,128)S(1)} fusion(f32[24,4,128,1]{2,3,1,0:T(1,128)S(1)} %bitcast.54, f32[24,4,128,128]{3,2,1,0:T(8,128)} %param.29), kind=kOutput, calls=%fused_computation.74 | convolution fusion | flops 3145728 | bytes 6389760 | tf_op jit(solution)/shard_map/shkv,shk->shv/dot_general | solution.py:80
  10.9 0.1 fusion.23
  11.0 0.6 copy-done.1
  11.6 3.8 %multiply_add_fusion = f32[24,4,128,128]{3,2,1,0:T(8,128)} fusion(f32[24,4,128,128]{3,2,1,0:T(8,128)S(1)} %copy-done.1, f32[24,4,128]{2,1,0:T(4,128)S(1)} %fusion.23, f32[24,4,128]{2,1,0:T(4,128)S(1)} %broadcast_multiply_fusion, f32[24,4]{1,0:T(8,128)S(1)} %copy.61), kind=kLoop, calls=%fused_computation | loop fusion | flops 4718592 | bytes 12681600 | tf_op jit(solution)/shard_map/add | solution.py:82
  15.5 0.4 fusion.3
  15.9 0.1 multiply_reduce_fusion.2
  16.2 3.9 %fusion.41 = f32[24,4,1,128]{3,2,1,0:T(1,128)S(1)} fusion(f32[24,4,128,128]{3,2,1,0:T(8,128)} %multiply_add_fusion, f32[24,4,128,1]{2,3,1,0:T(1,128)S(1)} %bitcast.57), kind=kOutput, calls=%fused_computation.75 | convolution fusion | flops 3145728 | bytes 6389760 | tf_op jit(solution)/shard_map/shkv,shk->shv/dot_general | solution.py:83
  20.2 0.4 fusion.2
  20.8 0.4 convolution_convert_fusion.2
  21.2 4.9 %all_to_all.28 = bf16[2,24,2048]{2,1,0:T(8,128)(2,1)S(1)} all-to-all(bf16[2,24,2048]{2,1,0:T(8,128)(2,1)S(1)} %broadcast_in_dim.4), channel_id=1, replica_groups=mesh['ep'=64,'tp'=2] {'tp'}, dimensions={0} | all-to-all | bytes 393216 | tf_op jit(solution)/shard_map/all_to_all | solution.py:11
  26.2 0.1 multiply_reduce_fusion
  27.0 0.2 select_reduce_fusion
  27.2 0.4 convolution_convert_fusion.1
  27.6 0.3 reshape.143
  28.0 23.5 %all_to_all.29 = bf16[64,1,2,2048]{3,2,1,0:T(2,128)(2,1)S(1)} all-to-all(bf16[64,1,2,2048]{3,2,1,0:T(2,128)(2,1)S(1)} %bitcast.51), channel_id=1, replica_groups=mesh['ep'=64,'tp'=2] {'ep'}, dimensions={0} | all-to-all | bytes 1048576 | tf_op jit(solution)/shard_map/all_to_all | solution.py:107
  51.5 0.2 reshape.144
  51.7 1.5 %fusion.15 = f32[128,256]{1,0:T(8,128)S(1)} fusion(bf16[128,2048]{1,0:T(8,128)(2,1)S(1)} %reshape.144, bf16[1,2048,256]{2,1,0:T(8,128)(2,1)} %param.33), kind=kOutput, calls=%fused_computation.27 | convolution fusion | flops 134217728 | bytes 1703936 | tf_op jit(solution)/shard_map/dot_general | solution.py:109
  53.2 1.5 %fusion.1 = bf16[128,256]{1,0:T(8,128)(2,1)S(1)} fusion(bf16[128,2048]{1,0:T(8,128)(2,1)S(1)} %reshape.144, bf16[1,2048,256]{2,1,0:T(8,128)(2,1)} %param.34, f32[128,256]{1,0:T(8,128)S(1)} %fusion.15), kind=kOutput, calls=%fused_computation.7 | convolution fusion | flops 134414336 | bytes 1769472 | tf_op jit(solution)/shard_map/dot_general | solution.py:110
  54.8 1.5 %convolution_convert_fusion = bf16[64,2,2048]{2,0,1:T(8,128)(2,1)S(1)} fusion(bf16[1,256,2048]{2,1,0:T(8,128)(2,1)} %param.35, bf16[64,2,256]{2,1,0:T(2,128)(2,1)S(1)} %dot_general.56), kind=kOutput, calls=%fused_computation.1 | convolution fusion | flops 134479872 | bytes 1638400 | tf_op jit(solution)/shard_map/dot_general | solution.py:112
  56.3 0.4 reshape.145
  56.8 5.6 %all_to_all.30 = bf16[2,1,64,2,1024]{4,2,3,1,0:T(8,128)(2,1)S(1)} all-to-all(bf16[2,1,64,2,1024]{4,2,3,1,0:T(8,128)(2,1)S(1)} %bitcast.52), channel_id=1, replica_groups=mesh['ep'=64,'tp'=2] {'tp'}, dimensions={0} | all-to-all | bytes 1048576 | tf_op jit(solution)/shard_map/all_to_all | solution.py:28
  62.6 1.0 %copy.70 = bf16[1,64,2,1024]{3,2,0,1:T(2,128)(2,1)} copy(bf16[1,64,2,1024]{3,1,2,0:T(8,128)(2,1)S(1)} %bitcast.53) | data formatting | bytes 524288 | tf_op jit(solution)/shard_map/reduce_sum | solution.py:29
  63.5 4.6 %all-to-all-start.3 = ((bf16[1,64,2,1024]{3,2,0,1:T(2,128)(2,1)}), bf16[1,64,2,1024]{3,2,0,1:T(2,128)(2,1)S(1)}, u32[]{:S(2)}, u32[]{:S(2)}) async-start(bf16[1,64,2,1024]{3,2,0,1:T(2,128)(2,1)} %copy.70), calls=%async_computation.3 | async-start | bytes 524288 | tf_op jit(solution)/shard_map/all_to_all | solution.py:115
  68.4 10.0 %all-to-all-done.3 = bf16[1,64,2,1024]{3,2,0,1:T(2,128)(2,1)S(1)} async-done(((bf16[1,64,2,1024]{3,2,0,1:T(2,128)(2,1)}), bf16[1,64,2,1024]{3,2,0,1:T(2,128)(2,1)S(1)}, u32[]{:S(2)}, u32[]{:S(2)}) %all-to-all-start.3) | async-done | bytes 262176 | tf_op jit(solution)/shard_map/all_to_all | solution.py:115
  78.4 0.2 fusion
  78.7 0.6 add_convert_fusion
  (60 shorter events, 2.0 us)
Async XLA Ops:
  0.6 20.2 %copy-start = (bf16[512,2048]{1,0:T(8,128)(2,1)S(1)}, bf16[512,2048]{1,0:T(8,128)(2,1)}, u32[]{:S(2)}) copy-start(bf16[512,2048]{1,0:T(8,128)(2,1)} %param.31) | copy-start | bytes 6291460
  0.6 3.6 %copy-start.2 = (bf16[24,2048]{1,0:T(8,128)(2,1)S(1)}, bf16[24,2048]{1,0:T(8,128)(2,1)}, u32[]{:S(2)}) copy-start(bf16[24,2048]{1,0:T(8,128)(2,1)} %param.19) | copy-start | bytes 294916
  0.7 3.6 %copy-start.5 = (f32[2048]{0:T(1024)S(1)}, f32[2048]{0:T(1024)}, u32[]{:S(2)}) copy-start(f32[2048]{0:T(1024)} %param.20) | copy-start | bytes 24580
  0.7 3.6 %copy-start.12 = (f32[4]{0:T(128)S(1)}, f32[4]{0:T(128)}, u32[]{:S(2)}) copy-start(f32[4]{0:T(128)} %param.27) | copy-start | bytes 52
  0.7 3.6 %copy-start.10 = (bf16[2048,4]{0,1:T(4,128)(2,1)S(1)}, bf16[2048,4]{0,1:T(4,128)(2,1)}, u32[]{:S(2)}) copy-start(bf16[2048,4]{0,1:T(4,128)(2,1)} %param.25) | copy-start | bytes 49156
  0.7 3.6 %copy-start.13 = (f32[4]{0:T(128)S(1)}, f32[4]{0:T(128)}, u32[]{:S(2)}) copy-start(f32[4]{0:T(128)} %param.28) | copy-start | bytes 52
  1.9 4.8 %copy-start.11 = (bf16[2048,4]{0,1:T(4,128)(2,1)S(1)}, bf16[2048,4]{0,1:T(4,128)(2,1)}, u32[]{:S(2)}) copy-start(bf16[2048,4]{0,1:T(4,128)(2,1)} %param.26) | copy-start | bytes 49156
  7.0 4.6 %copy-start.1 = (f32[24,4,128,128]{3,2,1,0:T(8,128)S(1)}, f32[24,4,128,128]{3,2,1,0:T(8,128)}, u32[]{:S(2)}) copy-start(f32[24,4,128,128]{3,2,1,0:T(8,128)} %param.29) | copy-start | bytes 18874372
  11.6 3.8 %copy-start.3 = (bf16[2048,512]{1,0:T(8,128)(2,1)S(1)}, bf16[2048,512]{1,0:T(8,128)(2,1)}, u32[]{:S(2)}) copy-start(bf16[2048,512]{1,0:T(8,128)(2,1)} %param.21) | copy-start | bytes 6291460
  16.2 4.0 %copy-start.4 = (bf16[2048,512]{1,0:T(8,128)(2,1)S(1)}, bf16[2048,512]{1,0:T(8,128)(2,1)}, u32[]{:S(2)}) copy-start(bf16[2048,512]{1,0:T(8,128)(2,1)} %param.24) | copy-start | bytes 6291460
  20.0 0.7 copy-start.9
  20.6 5.7 %copy-start.6 = (f32[2048]{0:T(1024)S(1)}, f32[2048]{0:T(1024)}, u32[]{:S(2)}) copy-start(f32[2048]{0:T(1024)} %param.32) | copy-start | bytes 24580
  20.8 5.8 %copy-start.7 = (s32[24,2]{0,1:T(2,128)S(1)}, s32[24,2]{0,1:T(2,128)}, u32[]{:S(2)}) copy-start(s32[24,2]{0,1:T(2,128)} %param.36) | copy-start | bytes 580
  56.7 21.7 %copy-start.8 = (f32[24,2]{0,1:T(2,128)S(1)}, f32[24,2]{0,1:T(2,128)}, u32[]{:S(2)}) copy-start(f32[24,2]{0,1:T(2,128)} %param.37) | copy-start | bytes 580
  63.5 14.8 %all-to-all-start.3 = ((bf16[1,64,2,1024]{3,2,0,1:T(2,128)(2,1)}), bf16[1,64,2,1024]{3,2,0,1:T(2,128)(2,1)S(1)}, u32[]{:S(2)}, u32[]{:S(2)}) async-start(bf16[1,64,2,1024]{3,2,0,1:T(2,128)(2,1)} %copy.70), calls=%async_computation.3 | async-start | bytes 524288 | tf_op jit(solution)/shard_map/all_to_all | solution.py:115
where the time goes:
time: 79.8 us; the launch traced here: 79.3 us
  blocking collectives  34.1 us (43%)
  matrix products  18.8 us (24%)
  waiting for transfers between devices  9.98 us (13%)
  other arithmetic  7.13 us (9%)
  starting transfers between devices  4.62 us (6%)
  local copies, waits for them, and re-layouts  3.68 us (5%)
  between operations  1.04 us (1%)
    all_to_all x1, blocking collectives, per_device(): lax.all_to_all(outgoing, 'ep', split_axis=0, concat_axis=1, tiled=True)  23.5 us
    all_to_all x1, waiting for transfers between devices, per_device(): lax.all_to_all(summed, 'ep', split_axis=1, concat_axis=0, tiled=True)  9.98 us
    all_to_all x1, blocking collectives, sum_at_owner(): lax.all_to_all(tiles, axis, split_axis=0, concat_axis=0, tiled=True)  5.63 us
    dot_general x6, matrix products, project(): jnp.dot(normed, weight, preferred_element_type=jnp.float32)  5.45 us
    all_to_all x1, blocking collectives, copy_for_each(): lax.all_to_all(jnp.broadcast_to(value[None], (peers, *value.shape)), axis...  4.92 us
    all_to_all x1, starting transfers between devices, per_device(): lax.all_to_all(summed, 'ep', split_axis=1, concat_axis=0, tiled=True)  4.62 us
    dot_general x1, matrix products, per_device(): predicted = jnp.einsum('shkv,shk->shv', state, key)  3.87 us
    dot_general x1, matrix products, per_device(): read = jnp.einsum('shkv,shk->shv', new_state, query)  3.86 us
  transfers between devices with their start and end apart: 1, of which 1 were waited for; matrix products, arithmetic and copies ran while one was open for 0% of the time, Pallas kernels for 0%

commit v1 on v0

v1 whole, which is shorter than its diff:
```python
import functools

import jax
import jax.numpy as jnp
from jax import lax
from jax.experimental import pallas as pl
from jax.experimental.pallas import tpu as pltpu
from jax.sharding import PartitionSpec as P

EPS = 1e-06
F32 = jnp.float32
BF16 = jnp.bfloat16
MESH = pl.DeviceIdType.MESH
LANES = 128


def rms_scale(rows, gain):
    return rows * lax.rsqrt(jnp.mean(rows * rows, axis=-1, keepdims=True) + EPS) * gain


def unit_rows(rows):
    return rows * lax.rsqrt(jnp.sum(rows * rows, axis=-1, keepdims=True) + EPS)


def silu(x):
    return x * (1.0 / (1.0 + jnp.exp(-x)))


def softplus(x):
    return jnp.maximum(x, 0.0) + jnp.log(1.0 + jnp.exp(-jnp.abs(x)))


def mixer_kernel(
    tok_h, gain_h, wq_h, wk_h, wv_h, wz_h, wd_h, wb_h, rate_h, bias_h, st_h, og_h, rt_h,
    ns_h, ho_ref, tab_ref,
    tok, gain, wbuf, wd, wb, rate, bias, st, og, rt, pq, wr, sem_small, sem_w, sem_s, sem_o,
):
    seqs = tok.shape[0]
    heads = st.shape[0]
    hd = st.shape[2]
    experts = 64

    small = [
        pltpu.make_async_copy(a, b, sem_small.at[i])
        for i, (a, b) in enumerate(
            [(tok_h, tok), (gain_h, gain), (wd_h, wd), (wb_h, wb), (rate_h, rate), (bias_h, bias), (og_h, og), (rt_h, rt)]
        )
    ]
    for c in small:
        c.start()
    w_in, s_in = [], []
    for h in range(heads):
        cols = pl.ds(h * hd, hd)
        w_in.append(
            [
                pltpu.make_async_copy(w.at[:, cols], wbuf.at[h, :, pl.ds(i * hd, hd)], sem_w.at[h, i])
                for i, w in enumerate((wq_h, wk_h, wv_h, wz_h))
            ]
        )
        s_in.append(pltpu.make_async_copy(st_h.at[:, h], st.at[h], sem_s.at[h]))
        for c in w_in[h]:
            c.start()
        s_in[h].start()
    for c in small:
        c.wait()

    ids = lax.broadcasted_iota(jnp.int32, (experts, seqs), 0)
    row = lax.broadcasted_iota(jnp.int32, (experts, seqs), 1)
    r = rt[...]
    hits = [ids == r[j : j + 1, :] for j in range(2)]
    either = hits[0] | hits[1]
    first = jnp.min(jnp.where(either, row, seqs), axis=1, keepdims=True)
    last = jnp.max(jnp.where(either, row, 0), axis=1, keepdims=True)
    first_row = jnp.where(first == seqs, 0, first)
    diag = lax.broadcasted_iota(jnp.int32, (experts, experts), 0) == lax.broadcasted_iota(
        jnp.int32, (experts, experts), 1
    )
    tab_ref[0:1, 0:experts] = jnp.sum(jnp.where(diag, first_row, 0), axis=0, keepdims=True)
    tab_ref[1:2, 0:experts] = jnp.sum(jnp.where(diag, last, 0), axis=0, keepdims=True)
    later = jnp.where(row > first, 1, 0)
    for j in range(2):
        slot = jnp.sum(jnp.where(hits[j], later, 0), axis=0, keepdims=True)
        tab_ref[2 + j : 3 + j, 0:seqs] = r[j : j + 1, :] * 2 + slot

    x = tok[...].astype(F32)
    normed = rms_scale(x, gain[...]).astype(BF16)
    normed32 = normed.astype(F32)

    def narrow(w, h):
        got = jnp.sum(normed32 * w[h : h + 1, :].astype(F32), axis=1, keepdims=True)
        return got.astype(BF16).astype(F32)

    fades, betas = [], []
    for h in range(heads):
        fade = jnp.exp(-rate[h] * softplus(narrow(wd, h) + bias[h]))
        fades.append(jnp.broadcast_to(fade, (seqs, hd)))
        betas.append(jnp.broadcast_to(1.0 / (1.0 + jnp.exp(-narrow(wb, h))), (seqs, hd)))

    out = []
    for h in range(heads):
        for c in w_in[h]:
            c.wait()
        raw = jnp.dot(normed, wbuf[h], preferred_element_type=F32).astype(BF16).astype(F32)
        q = unit_rows(silu(raw[:, 0:hd])) * hd ** (-0.5)
        k = unit_rows(silu(raw[:, hd : 2 * hd]))
        v = silu(raw[:, 2 * hd : 3 * hd])
        z = silu(raw[:, 3 * hd : 4 * hd])
        kq = jnp.sum(k * q, axis=1, keepdims=True)
        kt = k.T
        qt = q.T
        fade, beta = fades[h], betas[h]
        s_in[h].wait()
        for s in range(seqs):
            state = st[h, s]
            kcol = jnp.broadcast_to(kt[:, s : s + 1], (hd, hd))
            qcol = jnp.broadcast_to(qt[:, s : s + 1], (hd, hd))
            fade_s = fade[s : s + 1, :]
            pred = jnp.sum(state * kcol, axis=0, keepdims=True)
            pq[s : s + 1, :] = jnp.sum(state * qcol, axis=0, keepdims=True)
            written = beta[s : s + 1, :] * (v[s : s + 1, :] - fade_s * pred)
            wr[s : s + 1, :] = written
            st[h, s] = fade_s * state + kcol * written
            if s % 8 == 7:
                part = pl.ds(s - 7, 8)
                c = pltpu.make_async_copy(st.at[h, part], ns_h.at[part, h], sem_o.at[h, s // 8])
                c.start()
                out.append(c)
        read = fade * pq[...] + kq * wr[...]
        ho_ref[:, h * hd : (h + 1) * hd] = (rms_scale(read, og[...]) * z).astype(BF16)
    for c in out:
        c.wait()


def moe_kernel(
    n_ep, dims,
    ho_h, wo_h, tok_h, gain_h, eg_h, eu_h, ed_h, tab_ref, rw_ref,
    out_ref,
    ho, wo, tok, gain, wg, wu, wd, mix, mix_in, moe32, moe, send, recv, rows32, lhs, term32, rsend, ret, ret32, acc32, res,
    sem_l, sem_w, sem_x, sem_push, sem_pull, sem_send, sem_recv, sem_self, sem_back, sem_home, sem_bself,
):
    seqs, width = tok.shape
    half = width // 2
    tiles = width // LANES
    htiles = tiles // 2
    me = lax.axis_index("ep")
    core = lax.axis_index("tp")
    other = 1 - core
    par = lax.rem(me, 2)
    nz, ny, nx = dims

    loads = [
        pltpu.make_async_copy(a, b, sem_l.at[i])
        for i, (a, b) in enumerate([(ho_h, ho), (wo_h, wo), (tok_h, tok), (gain_h, gain)])
    ]
    for c in loads:
        c.start()
    wloads = [
        pltpu.make_async_copy(a, b.at[core], sem_w.at[i])
        for i, (a, b) in enumerate([(eg_h, wg), (eu_h, wu), (ed_h, wd)])
    ]
    for c in wloads:
        c.start()

    barrier = pltpu.get_barrier_semaphore()
    pl.semaphore_signal(barrier, inc=1, device_id={"ep": me, "tp": other}, device_id_type=MESH)

    def greet(j, _):
        d = lax.rem(me + j, n_ep)
        for t in range(2):
            pl.semaphore_signal(barrier, inc=1, device_id={"ep": d, "tp": t}, device_id_type=MESH)
        return 0

    lax.fori_loop(1, n_ep, greet, 0)

    loads[0].wait()
    loads[1].wait()
    mix[...] = jnp.dot(ho[...], wo[...], preferred_element_type=F32).astype(BF16)
    for c in loads[2:]:
        c.wait()
    pl.semaphore_wait(barrier, 2 * n_ep - 1)

    partner = {"ep": me, "tp": other}
    xchg = pltpu.make_async_remote_copy(
        mix, mix_in, sem_x.at[0], sem_x.at[1], device_id=partner, device_id_type=MESH
    )
    xchg.start()
    pushes = [
        pltpu.make_async_remote_copy(
            b.at[core], b.at[core], sem_push.at[i], sem_pull.at[i], device_id=partner, device_id_type=MESH
        )
        for i, b in enumerate((wg, wu, wd))
    ]
    wloads[0].wait()
    pushes[0].start()
    xchg.wait()

    resid = tok[...].astype(F32) + (mix[...].astype(F32) + mix_in[...].astype(F32))
    moe_in = rms_scale(resid, gain[...])
    for t in range(tiles):
        moe32[pl.ds(t, seqs, stride=tiles), :] = moe_in[:, t * LANES : (t + 1) * LANES]

    @pl.when(core == 0)
    def _():
        res[...] = resid[:, :half]

    @pl.when(core == 1)
    def _():
        res[...] = resid[:, half:]

    for t in range(seqs):
        moe[t] = moe32[t * tiles : (t + 1) * tiles, :].astype(BF16)
    for d in range(n_ep):
        send[d] = moe[tab_ref[core, d]]

    z0, y0, x0 = me // (ny * nx), lax.rem(me // nx, ny), lax.rem(me, nx)
    zs = [lax.rem(z0 + i, nz) * (ny * nx) for i in range(nz)]
    ys = [lax.rem(y0 + i, ny) * nx for i in range(ny)]
    xs = [lax.rem(x0 + i, nx) for i in range(nx)]
    hop = lambda i, n: min(i, n - i)
    order = sorted(
        [(a, b, c) for a in range(nz) for b in range(ny) for c in range(nx) if a or b or c],
        key=lambda o: -(hop(o[0], nz) + hop(o[1], ny) + hop(o[2], nx)),
    )
    my_row = core * (n_ep // 2) + me // 2
    for a, b, c in order:
        d = zs[a] + ys[b] + xs[c]
        pltpu.make_async_remote_copy(
            send.at[d], recv.at[my_row], sem_send, sem_recv, device_id={"ep": d, "tp": par}, device_id_type=MESH
        ).start()

    self_copy = pltpu.make_async_copy(send.at[me], recv.at[my_row], sem_recv)
    self_push = pltpu.make_async_remote_copy(
        send.at[me], recv.at[my_row], sem_self, sem_recv, device_id=partner, device_id_type=MESH
    )

    @pl.when(par == core)
    def _():
        self_copy.start()

    @pl.when(par != core)
    def _():
        self_push.start()

    for i in (1, 2):
        wloads[i].wait()
        pushes[i].start()

    pltpu.make_async_copy(recv, recv, sem_recv).wait()
    for t in range(n_ep):
        rows32[t * tiles : (t + 1) * tiles, :] = recv[t].astype(F32)
    for t in range(tiles):
        lhs[:, t * LANES : (t + 1) * LANES] = rows32[pl.ds(t, n_ep, stride=tiles), :].astype(BF16)
    pushes[0].wait()
    pushes[1].wait()
    hid = []
    for p in range(2):
        g = jnp.dot(lhs[...], wg[p], preferred_element_type=F32)
        u = jnp.dot(lhs[...], wu[p], preferred_element_type=F32)
        hid.append((silu(g) * u).astype(BF16))
    pushes[2].wait()
    for t in range(tiles):
        cols = slice(t * LANES, (t + 1) * LANES)
        got = jnp.dot(hid[0], wd[0, :, cols], preferred_element_type=F32) + jnp.dot(
            hid[1], wd[1, :, cols], preferred_element_type=F32
        )
        term32[pl.ds(t, n_ep, stride=tiles), :] = got
    for i in range(n_ep // 2):
        for hh in range(2):
            for s in range(2):
                at = (s * (n_ep // 2) + i) * tiles + hh * htiles
                rsend[hh, i, s] = term32[at : at + htiles, :].astype(BF16)

    mine = pl.ds(2 * me, 2)
    for a, b, c in order:
        if c % 2:
            continue
        d = zs[a] + ys[b] + lax.rem(x0 + jnp.where(par == core, c, c + 1), nx)
        for hh in range(2):
            pltpu.make_async_remote_copy(
                rsend.at[hh, d // 2], ret.at[mine], sem_back, sem_home, device_id={"ep": d, "tp": hh}, device_id_type=MESH
            ).start()
    last = zs[0] + ys[0] + lax.rem(x0 + jnp.where(par == core, 0, 1), nx)
    far = {"ep": last, "tp": other}
    back_other = pltpu.make_async_remote_copy(
        rsend.at[other, last // 2], ret.at[mine], sem_bself.at[0], sem_home, device_id=far, device_id_type=MESH
    )
    back_other.start()
    back_local = pltpu.make_async_copy(rsend.at[core, last // 2], ret.at[mine], sem_home)
    back_near = pltpu.make_async_remote_copy(
        rsend.at[core, last // 2], ret.at[mine], sem_bself.at[1], sem_home,
        device_id={"ep": last, "tp": core}, device_id_type=MESH,
    )

    @pl.when(par == core)
    def _():
        back_local.start()

    @pl.when(par != core)
    def _():
        back_near.start()

    pltpu.make_async_copy(send.at[pl.ds(0, n_ep - 1)], send.at[pl.ds(0, n_ep - 1)], sem_send).wait()

    @pl.when(par != core)
    def _():
        self_push.wait_send()

    pltpu.make_async_copy(ret, ret, sem_home).wait()
    for t in range(2 * n_ep):
        ret32[t] = ret[t].astype(F32)
    for t in range(seqs):
        acc = None
        for j in range(2):
            one = ret32[tab_ref[2 + j, t]] * rw_ref[j, t]
            acc = one if acc is None else acc + one
        acc32[t * htiles : (t + 1) * htiles, :] = acc
    for t in range(htiles):
        cols = slice(t * LANES, (t + 1) * LANES)
        out_ref[:, cols] = (res[:, cols] + acc32[pl.ds(t, seqs, stride=htiles), :]).astype(BF16)

    pltpu.make_async_copy(
        rsend.at[:, pl.ds(0, n_ep // 2 - 1)], rsend.at[:, pl.ds(0, n_ep // 2 - 1)], sem_back
    ).wait()
    back_other.wait_send()

    @pl.when(par != core)
    def _():
        back_near.wait_send()


HBM = pl.BlockSpec(memory_space=pltpu.HBM)
ANY = pl.BlockSpec(memory_space=pl.ANY)
VMEM = pl.BlockSpec(memory_space=pltpu.VMEM)
SMEM = pl.BlockSpec(memory_space=pltpu.SMEM)


def per_device(
    dims,
    tokens, attn_gain, w_query, w_key, w_value, w_zgate, w_decay, w_beta, decay_rate, decay_bias,
    state, out_gain, w_out, ffn_gain, expert_gate, expert_up, expert_down, routes, route_weight,
):
    seqs, width = tokens.shape
    heads, hd = state.shape[1], state.shape[2]
    n_ep = lax.axis_size("ep")
    tiles = width // LANES
    hidden = expert_gate.shape[2]
    dma = pltpu.SemaphoreType.DMA

    new_state, heads_out, table = pl.pallas_call(
        mixer_kernel,
        name="mixer",
        out_shape=(
            jax.ShapeDtypeStruct(state.shape, F32),
            jax.ShapeDtypeStruct((seqs, heads * hd), BF16),
            jax.ShapeDtypeStruct((8, LANES), jnp.int32),
        ),
        in_specs=[HBM] * 13,
        out_specs=(ANY, VMEM, VMEM),
        scratch_shapes=[
            pltpu.VMEM((seqs, width), BF16),
            pltpu.VMEM((1, width), F32),
            pltpu.VMEM((heads, width, 4 * hd), BF16),
            pltpu.VMEM((heads, width), BF16),
            pltpu.VMEM((heads, width), BF16),
            pltpu.SMEM((heads,), F32),
            pltpu.SMEM((heads,), F32),
            pltpu.VMEM((heads, seqs, hd, hd), F32),
            pltpu.VMEM((1, hd), F32),
            pltpu.VMEM((2, seqs), jnp.int32),
            pltpu.VMEM((seqs, hd), F32),
            pltpu.VMEM((seqs, hd), F32),
            dma((8,)),
            dma((heads, 4)),
            dma((heads,)),
            dma((heads, seqs // 8)),
        ],
        compiler_params=pltpu.CompilerParams(vmem_limit_bytes=24 * 2**20),
        cost_estimate=pl.CostEstimate(flops=10**8, bytes_accessed=2 * 10**7, transcendentals=0),
    )(
        tokens, attn_gain.reshape(1, width), w_query, w_key, w_value, w_zgate, w_decay.T, w_beta.T,
        decay_rate, decay_bias, state, out_gain.reshape(1, hd), routes.T,
    )

    layer_out = pl.pallas_call(
        functools.partial(moe_kernel, n_ep, dims),
        name="experts",
        out_shape=jax.ShapeDtypeStruct((seqs, width // 2), BF16),
        in_specs=[ANY, HBM, ANY, ANY, HBM, HBM, HBM, SMEM, SMEM],
        out_specs=VMEM,
        scratch_shapes=[
            pltpu.VMEM((seqs, heads * hd), BF16),
            pltpu.VMEM(w_out.shape, BF16),
            pltpu.VMEM((seqs, width), BF16),
            pltpu.VMEM((1, width), F32),
            pltpu.VMEM((2, width, hidden), BF16),
            pltpu.VMEM((2, width, hidden), BF16),
            pltpu.VMEM((2, hidden, width), BF16),
            pltpu.VMEM((seqs, width), BF16),
            pltpu.VMEM((seqs, width), BF16),
            pltpu.VMEM((seqs * tiles, LANES), F32),
            pltpu.VMEM((seqs, tiles, LANES), BF16),
            pltpu.VMEM((n_ep, tiles, LANES), BF16),
            pltpu.VMEM((n_ep, tiles, LANES), BF16),
            pltpu.VMEM((n_ep * tiles, LANES), F32),
            pltpu.VMEM((n_ep, width), BF16),
            pltpu.VMEM((n_ep * tiles, LANES), F32),
            pltpu.VMEM((2, n_ep // 2, 2, tiles // 2, LANES), BF16),
            pltpu.VMEM((2 * n_ep, tiles // 2, LANES), BF16),
            pltpu.VMEM((2 * n_ep, tiles // 2, LANES), F32),
            pltpu.VMEM((seqs * tiles // 2, LANES), F32),
            pltpu.VMEM((seqs, width // 2), F32),
            dma((4,)),
            dma((3,)),
            dma((2,)),
            dma((3,)),
            dma((3,)),
            dma,
            dma,
            dma,
            dma,
            dma,
            dma((2,)),
        ],
        compiler_params=pltpu.CompilerParams(
            collective_id=0, has_side_effects=True, vmem_limit_bytes=24 * 2**20
        ),
        cost_estimate=pl.CostEstimate(flops=10**8, bytes_accessed=10**7, transcendentals=0),
    )(
        heads_out, w_out, tokens, ffn_gain.reshape(1, width), expert_gate[0], expert_up[0],
        expert_down[0], table, route_weight.T,
    )
    return (layer_out, new_state)


def solution(mesh):
    in_specs = (
        P("ep", None), P(), P(None, "tp"), P(None, "tp"), P(None, "tp"), P(None, "tp"), P(None, "tp"), P(None, "tp"),
        P("tp"), P("tp"), P("ep", "tp", None, None), P(), P("tp", None), P(), P("ep", None, "tp"), P("ep", None, "tp"),
        P("ep", "tp", None), P("ep", None), P("ep", None),
    )
    out_specs = (P("ep", "tp"), P("ep", "tp", None, None))
    side = round(mesh.shape["ep"] ** (1 / 3))
    dims = (side, side, side)
    return jax.shard_map(
        functools.partial(per_device, dims), mesh=mesh, in_specs=in_specs, out_specs=out_specs, check_vma=False
    )
```

time: 79.8 us -> 55.8 us (0.70)
  Pallas kernels: 0 us -> 39.1 us
  blocking collectives: 34.1 us -> 0 us
  matrix products: 18.8 us -> 0 us
  local copies, waits for them, and re-layouts: 3.68 us -> 15.5 us
  waiting for transfers between devices: 9.98 us -> 0 us
  other arithmetic: 7.13 us -> 0 us
  starting transfers between devices: 4.62 us -> 0 us
    pallas_call x0 -> x2, Pallas kernels: none -> 39.1 us  [the longest x1 28.6 us: per_device(): pl.pallas_call(functools.partial(moe_kernel, n_ep, dims), name='experts',...]
    all_to_all x3 -> x0, blocking collectives: 34.1 us -> none  [the longest x1 23.5 us: per_device(): lax.all_to_all(outgoing, 'ep', split_axis=0, concat_axis=1, tiled=True)]
    dot_general x14 -> x0, matrix products: 18.8 us -> none  [the longest x6 5.45 us: project(): jnp.dot(normed, weight, preferred_element_type=jnp.float32)]
    unnamed x29 -> x39, local copies, waits for them, and re-layouts: 0.83 us -> 15.5 us
    all_to_all x1 -> x0, waiting for transfers between devices: 9.98 us -> none  [per_device(): lax.all_to_all(summed, 'ep', split_axis=1, concat_axis=0, tiled=True)]
    all_to_all x1 -> x0, starting transfers between devices: 4.62 us -> none  [per_device(): lax.all_to_all(summed, 'ep', split_axis=1, concat_axis=0, tiled=True)]
    add x3 -> x0, other arithmetic: 3.85 us -> none  [the longest x1 3.84 us: per_device(): fade[..., None, None] * state + key[..., :, None] * written[..., None, :]]
    reduce_sum x8 -> x0, other arithmetic: 1.95 us -> none  [the longest x3 1.42 us: rms_scale(): jnp.mean(rows * rows, axis=-1, keepdims=True) + EPS]
  transfers between devices with their start and end apart: 1 -> 0, of which waited for: 1 -> 0; matrix products, arithmetic and copies ran while one was open for 0% -> 0% of each run, Pallas kernels for 0% -> 0%
where the time goes in v1:
time: 55.8 us; the launch traced here: 55.3 us
  Pallas kernels  39.1 us (70%)
  local copies, waits for them, and re-layouts  15.5 us (28%)
  between operations  0.74 us (1%)
    pallas_call x1, Pallas kernels, per_device(): pl.pallas_call(functools.partial(moe_kernel, n_ep, dims), name='experts',...  28.6 us
    unnamed x39, local copies, waits for them, and re-layouts  15.5 us
    pallas_call x1, Pallas kernels, per_device(): pl.pallas_call(mixer_kernel, name='mixer', out_shape=(jax.ShapeDtypeStruc...  10.6 us

profile of v1, /device:TPU:1, one launch (start us, length us, event | category | flops | bytes accessed | tf_op | source)
XLA Modules:
  0.0 55.3 jit_solution(6319863903851970178)
XLA Ops:
  0.6 0.0 copy-start
  0.6 2.8 %copy-done = f32[24,4,128,128]{3,2,1,0:T(8,128)S(1)} copy-done((f32[24,4,128,128]{3,2,1,0:T(8,128)S(1)}, f32[24,4,128,128]{3,2,1,0:T(8,128)}, u32[]{:S(2)}) %copy-start) | copy-done | bytes 6291480
  3.4 0.0 copy-start.2
  3.4 1.6 %copy-done.2 = bf16[2048,512]{1,0:T(8,128)(2,1)S(1)} copy-done((bf16[2048,512]{1,0:T(8,128)(2,1)S(1)}, bf16[2048,512]{1,0:T(8,128)(2,1)}, u32[]{:S(2)}) %copy-start.2) | copy-done | bytes 2097176
  5.0 0.0 copy-start.3
  5.0 1.6 %copy-done.3 = bf16[2048,512]{1,0:T(8,128)(2,1)S(1)} copy-done((bf16[2048,512]{1,0:T(8,128)(2,1)S(1)}, bf16[2048,512]{1,0:T(8,128)(2,1)}, u32[]{:S(2)}) %copy-start.3) | copy-done | bytes 2097176
  6.6 0.0 copy-start.4
  6.6 1.6 %copy-done.4 = bf16[2048,512]{1,0:T(8,128)(2,1)S(1)} copy-done((bf16[2048,512]{1,0:T(8,128)(2,1)S(1)}, bf16[2048,512]{1,0:T(8,128)(2,1)}, u32[]{:S(2)}) %copy-start.4) | copy-done | bytes 2097176
  8.2 0.0 copy-start.5
  8.2 1.6 %copy-done.5 = bf16[2048,512]{1,0:T(8,128)(2,1)S(1)} copy-done((bf16[2048,512]{1,0:T(8,128)(2,1)S(1)}, bf16[2048,512]{1,0:T(8,128)(2,1)}, u32[]{:S(2)}) %copy-start.5) | copy-done | bytes 2097176
  9.8 0.0 copy-start.9
  9.8 0.9 %copy-done.9 = bf16[24,2048]{1,0:T(8,128)(2,1)S(1)} copy-done((bf16[24,2048]{1,0:T(8,128)(2,1)S(1)}, bf16[24,2048]{1,0:T(8,128)(2,1)}, u32[]{:S(2)}) %copy-start.9) | copy-done | bytes 98328
  10.7 0.0 copy-start.10
  10.7 0.7 %copy-done.10 = bf16[2048,4]{0,1:T(4,128)(2,1)S(1)} copy-done((bf16[2048,4]{0,1:T(4,128)(2,1)S(1)}, bf16[2048,4]{0,1:T(4,128)(2,1)}, u32[]{:S(2)}) %copy-start.10) | copy-done | bytes 16408
  11.4 0.0 copy-start.11
  11.4 0.7 %copy-done.11 = bf16[2048,4]{0,1:T(4,128)(2,1)S(1)} copy-done((bf16[2048,4]{0,1:T(4,128)(2,1)S(1)}, bf16[2048,4]{0,1:T(4,128)(2,1)}, u32[]{:S(2)}) %copy-start.11) | copy-done | bytes 16408
  12.1 0.7 %copy-done.12 = f32[2048]{0:T(1024)S(1)} copy-done((f32[2048]{0:T(1024)S(1)}, f32[2048]{0:T(1024)}, u32[]{:S(2)}) %copy-start.12) | copy-done | bytes 8216
  12.8 0.7 %copy-done.14 = s32[24,2]{0,1:T(2,128)S(1)} copy-done((s32[24,2]{0,1:T(2,128)S(1)}, s32[24,2]{0,1:T(2,128)}, u32[]{:S(2)}) %copy-start.14) | copy-done | bytes 216
  13.5 0.7 %copy-done.16 = f32[4]{0:T(128)S(1)} copy-done((f32[4]{0:T(128)S(1)}, f32[4]{0:T(128)}, u32[]{:S(2)}) %copy-start.16) | copy-done | bytes 40
  14.2 0.7 %copy-done.17 = f32[4]{0:T(128)S(1)} copy-done((f32[4]{0:T(128)S(1)}, f32[4]{0:T(128)}, u32[]{:S(2)}) %copy-start.17) | copy-done | bytes 40
  14.8 0.7 %copy-done.18 = f32[128]{0:T(128)S(1)} copy-done((f32[128]{0:T(128)S(1)}, f32[128]{0:T(128)}, u32[]{:S(2)}) %copy-start.18) | copy-done | bytes 536
  15.5 0.0 copy-start.13
  15.5 0.0 copy-start.15
  15.5 10.6 %mixer.1 = (f32[24,4,128,128]{3,2,1,0:T(8,128)}, bf16[24,512]{1,0:T(8,128)(2,1)S(1)}, s32[8,128]{1,0:T(8,128)S(1)}) custom-call(bf16[24,2048]{1,0:T(8,128)(2,1)S(1)} %copy-done.9, f32[1,2048]{1,0:T(1,128)S(1)} %bitcast.15, bf16[2048,512]{1,0:T(8,128)(2,1)S(1)} %copy-done.2, bf16[2048,512]{1,0:T(8,128)(2,1)S(1)} %copy-done.3, ...), custom_call_target="tpu_custom_call" | custom-call | flops 100000000 | bytes 20000000 | tf_op jit(solution)/shard_map/mixer/pallas_call | solution.py:349
  26.1 0.0 copy-done.1
  26.1 0.0 copy-done.6
  26.1 0.0 copy-done.7
  26.1 0.0 copy-done.8
  26.1 0.0 copy-done.13
  26.1 0.0 copy-done.15
  26.1 28.6 %experts.1 = bf16[24,1024]{1,0:T(8,128)(2,1)S(1)} custom-call(bf16[24,512]{1,0:T(8,128)(2,1)S(1)} %get-tuple-element.5.ho_h, bf16[512,2048]{1,0:T(8,128)(2,1)S(1)} %copy-done.1, bf16[24,2048]{1,0:T(8,128)(2,1)S(1)} %copy-done.9, f32[1,2048]{1,0:T(1,128)S(1)} %bitcast.16, bf16[2048,256]{1,0:T(8,128)(2,1)S(1)} %bitcast.10, bf16[2048,256]{1,0:T(8,128)(2,1)S(1)} %bitcast.11, ...), custom_call_target="tpu_custom_call" | custom-call | flops 100000000 | bytes 10000000 | tf_op jit(solution)/shard_map/experts/pallas_call | solution.py:384
  54.7 0.6 %copy.22 = bf16[24,1024]{1,0:T(8,128)(2,1)} copy(bf16[24,1024]{1,0:T(8,128)(2,1)S(1)} %experts.1) | data formatting | bytes 98304
  (9 shorter events, 0.0 us)
Async XLA Ops:
  0.6 2.8 %copy-start = (f32[24,4,128,128]{3,2,1,0:T(8,128)S(1)}, f32[24,4,128,128]{3,2,1,0:T(8,128)}, u32[]{:S(2)}) copy-start(f32[24,4,128,128]{3,2,1,0:T(8,128)} %st_h.1) | copy-start | bytes 18874372
  3.4 1.6 %copy-start.2 = (bf16[2048,512]{1,0:T(8,128)(2,1)S(1)}, bf16[2048,512]{1,0:T(8,128)(2,1)}, u32[]{:S(2)}) copy-start(bf16[2048,512]{1,0:T(8,128)(2,1)} %wq_h.1) | copy-start | bytes 6291460
  5.0 1.6 %copy-start.3 = (bf16[2048,512]{1,0:T(8,128)(2,1)S(1)}, bf16[2048,512]{1,0:T(8,128)(2,1)}, u32[]{:S(2)}) copy-start(bf16[2048,512]{1,0:T(8,128)(2,1)} %wk_h.1) | copy-start | bytes 6291460
  6.6 1.6 %copy-start.4 = (bf16[2048,512]{1,0:T(8,128)(2,1)S(1)}, bf16[2048,512]{1,0:T(8,128)(2,1)}, u32[]{:S(2)}) copy-start(bf16[2048,512]{1,0:T(8,128)(2,1)} %wv_h.1) | copy-start | bytes 6291460
  8.2 1.6 %copy-start.5 = (bf16[2048,512]{1,0:T(8,128)(2,1)S(1)}, bf16[2048,512]{1,0:T(8,128)(2,1)}, u32[]{:S(2)}) copy-start(bf16[2048,512]{1,0:T(8,128)(2,1)} %wz_h.1) | copy-start | bytes 6291460
  9.8 0.9 %copy-start.9 = (bf16[24,2048]{1,0:T(8,128)(2,1)S(1)}, bf16[24,2048]{1,0:T(8,128)(2,1)}, u32[]{:S(2)}) copy-start(bf16[24,2048]{1,0:T(8,128)(2,1)} %tok_h.3) | copy-start | bytes 294916
  10.7 0.7 %copy-start.10 = (bf16[2048,4]{0,1:T(4,128)(2,1)S(1)}, bf16[2048,4]{0,1:T(4,128)(2,1)}, u32[]{:S(2)}) copy-start(bf16[2048,4]{0,1:T(4,128)(2,1)} %param.25) | copy-start | bytes 49156
  11.4 0.7 %copy-start.11 = (bf16[2048,4]{0,1:T(4,128)(2,1)S(1)}, bf16[2048,4]{0,1:T(4,128)(2,1)}, u32[]{:S(2)}) copy-start(bf16[2048,4]{0,1:T(4,128)(2,1)} %param.26) | copy-start | bytes 49156
  12.1 0.7 %copy-start.12 = (f32[2048]{0:T(1024)S(1)}, f32[2048]{0:T(1024)}, u32[]{:S(2)}) copy-start(f32[2048]{0:T(1024)} %param.20) | copy-start | bytes 24580
  12.8 0.7 %copy-start.14 = (s32[24,2]{0,1:T(2,128)S(1)}, s32[24,2]{0,1:T(2,128)}, u32[]{:S(2)}) copy-start(s32[24,2]{0,1:T(2,128)} %param.36) | copy-start | bytes 580
  13.5 0.7 %copy-start.16 = (f32[4]{0:T(128)S(1)}, f32[4]{0:T(128)}, u32[]{:S(2)}) copy-start(f32[4]{0:T(128)} %rate_h.1) | copy-start | bytes 52
  14.2 0.7 %copy-start.17 = (f32[4]{0:T(128)S(1)}, f32[4]{0:T(128)}, u32[]{:S(2)}) copy-start(f32[4]{0:T(128)} %bias_h.1) | copy-start | bytes 52
  14.8 0.7 %copy-start.18 = (f32[128]{0:T(128)S(1)}, f32[128]{0:T(128)}, u32[]{:S(2)}) copy-start(f32[128]{0:T(128)} %param.30) | copy-start | bytes 1540
  15.5 10.6 %copy-start.1 = (bf16[512,2048]{1,0:T(8,128)(2,1)S(1)}, bf16[512,2048]{1,0:T(8,128)(2,1)}, u32[]{:S(2)}) copy-start(bf16[512,2048]{1,0:T(8,128)(2,1)} %wo_h.1) | copy-start | bytes 6291460
  15.5 10.6 %copy-start.6 = (bf16[1,2048,256]{2,1,0:T(8,128)(2,1)S(1)}, bf16[1,2048,256]{2,1,0:T(8,128)(2,1)}, u32[]{:S(2)}) copy-start(bf16[1,2048,256]{2,1,0:T(8,128)(2,1)} %param.33) | copy-start | bytes 3145732
  15.5 10.6 %copy-start.7 = (bf16[1,2048,256]{2,1,0:T(8,128)(2,1)S(1)}, bf16[1,2048,256]{2,1,0:T(8,128)(2,1)}, u32[]{:S(2)}) copy-start(bf16[1,2048,256]{2,1,0:T(8,128)(2,1)} %param.34) | copy-start | bytes 3145732
  15.5 10.6 %copy-start.8 = (bf16[1,256,2048]{2,1,0:T(8,128)(2,1)S(1)}, bf16[1,256,2048]{2,1,0:T(8,128)(2,1)}, u32[]{:S(2)}) copy-start(bf16[1,256,2048]{2,1,0:T(8,128)(2,1)} %param.35) | copy-start | bytes 3145732
  15.5 10.6 %copy-start.13 = (f32[2048]{0:T(1024)S(1)}, f32[2048]{0:T(1024)}, u32[]{:S(2)}) copy-start(f32[2048]{0:T(1024)} %param.32) | copy-start | bytes 24580
  15.5 10.6 %copy-start.15 = (f32[24,2]{0,1:T(2,128)S(1)}, f32[24,2]{0,1:T(2,128)}, u32[]{:S(2)}) copy-start(f32[24,2]{0,1:T(2,128)} %param.37) | copy-start | bytes 580

commit v2 on v1

--- a/solution.py
+++ b/solution.py
@@ -334,6 +334,10 @@
 SMEM = pl.BlockSpec(memory_space=pltpu.SMEM)
 
 
+def keep(a):
+    return pltpu.with_memory_space_constraint(a, pltpu.HBM)
+
+
 def per_device(
     dims,
     tokens, attn_gain, w_query, w_key, w_value, w_zgate, w_decay, w_beta, decay_rate, decay_bias,
@@ -377,8 +381,13 @@
         compiler_params=pltpu.CompilerParams(vmem_limit_bytes=24 * 2**20),
         cost_estimate=pl.CostEstimate(flops=10**8, bytes_accessed=2 * 10**7, transcendentals=0),
     )(
-        tokens, attn_gain.reshape(1, width), w_query, w_key, w_value, w_zgate, w_decay.T, w_beta.T,
-        decay_rate, decay_bias, state, out_gain.reshape(1, hd), routes.T,
+        *[
+            keep(a)
+            for a in (
+                tokens, attn_gain.reshape(1, width), w_query, w_key, w_value, w_zgate, w_decay.T, w_beta.T,
+                decay_rate, decay_bias, state, out_gain.reshape(1, hd), routes.T,
+            )
+        ]
     )
 
     layer_out = pl.pallas_call(
@@ -426,8 +435,8 @@
         ),
         cost_estimate=pl.CostEstimate(flops=10**8, bytes_accessed=10**7, transcendentals=0),
     )(
-        heads_out, w_out, tokens, ffn_gain.reshape(1, width), expert_gate[0], expert_up[0],
-        expert_down[0], table, route_weight.T,
+        heads_out, keep(w_out), keep(tokens), ffn_gain.reshape(1, width), keep(expert_gate[0]), keep(expert_up[0]),
+        keep(expert_down[0]), table, route_weight.T,
     )
     return (layer_out, new_state)
 

time: 55.8 us -> 42.7 us (0.77)
  local copies, waits for them, and re-layouts: 15.5 us -> 0.63 us
  Pallas kernels: 39.1 us -> 41.2 us
    unnamed x39 -> x5, local copies, waits for them, and re-layouts: 15.5 us -> 0.63 us
    pallas_call x1, Pallas kernels: 10.6 us -> 13.1 us  [per_device(): pl.pallas_call(mixer_kernel, name='mixer', out_shape=(jax.ShapeDtypeStruc...]
where the time goes in v2:
time: 42.7 us; the launch traced here: 42.6 us
  Pallas kernels  41.2 us (96%)
  between operations  0.68 us (2%)
  local copies, waits for them, and re-layouts  0.63 us (1%)
    pallas_call x1, Pallas kernels, per_device(): pl.pallas_call(functools.partial(moe_kernel, n_ep, dims), name='experts',...  28.2 us
    pallas_call x1, Pallas kernels, per_device(): pl.pallas_call(mixer_kernel, name='mixer', out_shape=(jax.ShapeDtypeStruc...  13.1 us

profile of v2, /device:TPU:1, one launch (start us, length us, event | category | flops | bytes accessed | tf_op | source)
XLA Modules:
  0.0 42.6 jit_solution(1117575990683732873)
XLA Ops:
  0.6 0.0 copy-start
  0.6 0.0 copy-start.1
  0.7 13.1 %mixer.1 = (f32[24,4,128,128]{3,2,1,0:T(8,128)}, bf16[24,512]{1,0:T(8,128)(2,1)S(1)}, s32[8,128]{1,0:T(8,128)S(1)}) custom-call(bf16[24,2048]{1,0:T(8,128)(2,1)} %tok_h.3, f32[1,2048]{1,0:T(1,128)} %bitcast.17, bf16[2048,512]{1,0:T(8,128)(2,1)} %wq_h.1, bf16[2048,512]{1,0:T(8,128)(2,1)} %wk_h.1, bf16[2048,512]{1,0:T(8,128)(2,1)} %wv_h.1, ...), custom_call_target="tpu_custom_call" | custom-call | flops 100000000 | bytes 20000000 | tf_op jit(solution)/shard_map/mixer/pallas_call | solution.py:353
  13.7 0.0 copy-done
  13.8 0.0 copy-done.1
  13.8 28.2 %experts.1 = bf16[24,1024]{1,0:T(8,128)(2,1)S(1)} custom-call(bf16[24,512]{1,0:T(8,128)(2,1)S(1)} %get-tuple-element.5.ho_h, bf16[512,2048]{1,0:T(8,128)(2,1)} %wo_h.1, bf16[24,2048]{1,0:T(8,128)(2,1)} %tok_h.3, f32[1,2048]{1,0:T(1,128)S(1)} %bitcast.10, bf16[2048,256]{1,0:T(8,128)(2,1)} %bitcast.12, bf16[2048,256]{1,0:T(8,128)(2,1)} %bitcast.13, ...), custom_call_target="tpu_custom_call" | custom-call | flops 100000000 | bytes 10000000 | tf_op jit(solution)/shard_map/experts/pallas_call | solution.py:393
  41.9 0.6 %copy.22 = bf16[24,1024]{1,0:T(8,128)(2,1)} copy(bf16[24,1024]{1,0:T(8,128)(2,1)S(1)} %experts.1) | data formatting | bytes 98304
Async XLA Ops:
  0.6 13.1 %copy-start = (f32[2048]{0:T(1024)S(1)}, f32[2048]{0:T(1024)}, u32[]{:S(2)}) copy-start(f32[2048]{0:T(1024)} %param.32) | copy-start | bytes 24580
  0.6 13.1 %copy-start.1 = (f32[24,2]{0,1:T(2,128)S(1)}, f32[24,2]{0,1:T(2,128)}, u32[]{:S(2)}) copy-start(f32[24,2]{0,1:T(2,128)} %param.37) | copy-start | bytes 580

commit v3 on v1

v3 whole, which is shorter than its diff:
```python
import functools

import jax
import jax.numpy as jnp
from jax import lax
from jax.experimental import pallas as pl
from jax.experimental.pallas import tpu as pltpu
from jax.sharding import PartitionSpec as P

EPS = 1e-06
F32 = jnp.float32
BF16 = jnp.bfloat16
MESH = pl.DeviceIdType.MESH
LANES = 128


def rms_scale(rows, gain):
    return rows * lax.rsqrt(jnp.mean(rows * rows, axis=-1, keepdims=True) + EPS) * gain


def unit_rows(rows):
    return rows * lax.rsqrt(jnp.sum(rows * rows, axis=-1, keepdims=True) + EPS)


def silu(x):
    return x * (1.0 / (1.0 + jnp.exp(-x)))


def softplus(x):
    return jnp.maximum(x, 0.0) + jnp.log(1.0 + jnp.exp(-jnp.abs(x)))


def layer_kernel(
    n_ep, dims,
    tok_h, gain_h, wq_h, wk_h, wv_h, wz_h, wd_h, wb_h, rate_h, bias_h, st_h, og_h, wo_h, fgain_h, eg_h, eu_h, ed_h, rt_h, rw_h,
    out_ref, ns_ref,
    tok, gain, wbuf, wd, wb, rate, bias, og, wo, fgain, rt, rw, tab_v, tab,
    kts, written, fades, ho,
    wg, wu, wdn, mix, mix_in, moe32, moe, send, recv, rows32, lhs, term32, rsend, ret, ret32, acc32, res,
    sem_small, sem_w, sem_s, sem_wo, sem_tab, sem_e, sem_x, sem_push, sem_pull, sem_send, sem_recv, sem_self, sem_back, sem_home, sem_bself,
):
    seqs, width = tok.shape
    heads, hd = kts.shape[0], kts.shape[1]
    half = width // 2
    tiles = width // LANES
    htiles = tiles // 2
    me = lax.axis_index("ep")
    core = lax.axis_index("tp")
    other = 1 - core
    par = lax.rem(me, 2)
    shift = jnp.where(par == core, 0, 1)
    nz, ny, nx = dims

    small = [
        pltpu.make_async_copy(a, b, sem_small.at[i])
        for i, (a, b) in enumerate(
            [
                (tok_h, tok), (gain_h, gain), (wd_h, wd), (wb_h, wb), (rate_h, rate), (bias_h, bias), (og_h, og),
                (rt_h, rt), (fgain_h, fgain), (rw_h, rw),
            ]
        )
    ]
    for c in small:
        c.start()
    big = []
    for h in range(heads):
        cols = pl.ds(h * hd, hd)
        big.append(
            [
                pltpu.make_async_copy(w.at[:, cols], wbuf.at[h, :, pl.ds(i * hd, hd)], sem_w.at[h, i])
                for i, w in enumerate((wq_h, wk_h, wv_h, wz_h))
            ]
            + [pltpu.make_async_copy(st_h.at[:, h], ns_ref.at[:, h], sem_s.at[h])]
        )
    wo_in = pltpu.make_async_copy(wo_h, wo, sem_wo)
    e_in = [
        pltpu.make_async_copy(a, b.at[core], sem_e.at[i])
        for i, (a, b) in enumerate([(eg_h, wg), (eu_h, wu), (ed_h, wdn)])
    ]
    for c in big[0]:
        c.start()

    z0, y0, x0 = me // (ny * nx), lax.rem(me // nx, ny), lax.rem(me, nx)
    zs = [lax.rem(z0 + i, nz) * (ny * nx) for i in range(nz)]
    ys = [lax.rem(y0 + i, ny) * nx for i in range(ny)]
    xs = [lax.rem(x0 + i, nx) for i in range(nx)]
    xp = [lax.rem(x0 + i + shift, nx) for i in range(nx)]
    hop = lambda i, n: min(i, n - i)
    order = sorted(
        [(a, b, c) for a in range(nz) for b in range(ny) for c in range(nx)],
        key=lambda o: -(hop(o[0], nz) + hop(o[1], ny) + hop(o[2], nx)),
    )
    partner = {"ep": me, "tp": other}

    barrier = pltpu.get_barrier_semaphore()
    for a, b, c in order[:-1]:
        pl.semaphore_signal(
            barrier, inc=1, device_id={"ep": zs[a] + ys[b] + xs[c], "tp": par}, device_id_type=MESH
        )
        if c % 2 == 0:
            pl.semaphore_signal(
                barrier, inc=1, device_id={"ep": zs[a] + ys[b] + xp[c], "tp": 1 - par}, device_id_type=MESH
            )

    @pl.when(par != core)
    def _():
        pl.semaphore_signal(
            barrier, inc=1, device_id={"ep": zs[0] + ys[0] + xp[0], "tp": 1 - par}, device_id_type=MESH
        )

    pl.semaphore_signal(barrier, inc=1, device_id=partner, device_id_type=MESH)

    for c in small:
        c.wait()
    for c in big[1]:
        c.start()

    ids = lax.broadcasted_iota(jnp.int32, (n_ep, seqs), 0)
    row = lax.broadcasted_iota(jnp.int32, (n_ep, seqs), 1)
    r = rt[...]
    hits = [ids == r[j : j + 1, :] for j in range(2)]
    either = hits[0] | hits[1]
    first = jnp.min(jnp.where(either, row, seqs), axis=1, keepdims=True)
    last = jnp.max(jnp.where(either, row, 0), axis=1, keepdims=True)
    first_row = jnp.where(first == seqs, 0, first)
    diag = lax.broadcasted_iota(jnp.int32, (n_ep, n_ep), 0) == lax.broadcasted_iota(jnp.int32, (n_ep, n_ep), 1)
    tab_v[0:1, 0:n_ep] = jnp.sum(jnp.where(diag, first_row, 0), axis=0, keepdims=True)
    tab_v[1:2, 0:n_ep] = jnp.sum(jnp.where(diag, last, 0), axis=0, keepdims=True)
    later = jnp.where(row > first, 1, 0)
    for j in range(2):
        slot = jnp.sum(jnp.where(hits[j], later, 0), axis=0, keepdims=True)
        tab_v[2 + j : 3 + j, 0:seqs] = r[j : j + 1, :] * 2 + slot

    x = tok[...].astype(F32)
    normed = rms_scale(x, gain[...]).astype(BF16)
    normed32 = normed.astype(F32)

    def narrow(w, h):
        got = jnp.sum(normed32 * w[h : h + 1, :].astype(F32), axis=1, keepdims=True)
        return got.astype(BF16).astype(F32)

    betas = []
    for h in range(heads):
        fade = jnp.exp(-rate[h] * softplus(narrow(wd, h) + bias[h]))
        fades[h] = jnp.broadcast_to(fade, (seqs, hd))
        betas.append(jnp.broadcast_to(1.0 / (1.0 + jnp.exp(-narrow(wb, h))), (seqs, hd)))

    tab_copy = pltpu.make_async_copy(tab_v, tab, sem_tab)
    tab_copy.start()

    sub = lax.broadcasted_iota(jnp.int32, (8, hd), 0)
    for h in range(heads):
        for c in big[h]:
            c.wait()
        if h + 2 < heads:
            for c in big[h + 2]:
                c.start()
        if h + 2 == heads:
            wo_in.start()
        if h + 1 == heads:
            for c in e_in:
                c.start()
        raw = jnp.dot(normed, wbuf[h], preferred_element_type=F32).astype(BF16).astype(F32)
        q = unit_rows(silu(raw[:, 0:hd])) * hd ** (-0.5)
        k = unit_rows(silu(raw[:, hd : 2 * hd]))
        v = silu(raw[:, 2 * hd : 3 * hd])
        z = silu(raw[:, 3 * hd : 4 * hd])
        kq = jnp.sum(k * q, axis=1, keepdims=True)
        kts[h] = k.T
        preds, sqs = [], []
        for g in range(seqs // 8):
            pair = jnp.concatenate([k[g * 8 : g * 8 + 8], q[g * 8 : g * 8 + 8]], axis=0).astype(BF16)
            pred = sq = None
            for s in range(0, 8, 2):
                both = jnp.concatenate([ns_ref[g * 8 + s, h], ns_ref[g * 8 + s + 1, h]], axis=1).astype(BF16)
                got = jnp.dot(pair, both, preferred_element_type=F32)
                for i in range(2):
                    one, two = got[0:8, i * hd : (i + 1) * hd], got[8:16, i * hd : (i + 1) * hd]
                    pred = one if pred is None else jnp.where(sub == s + i, one, pred)
                    sq = two if sq is None else jnp.where(sub == s + i, two, sq)
            preds.append(pred)
            sqs.append(sq)
        pred, sq = jnp.concatenate(preds, axis=0), jnp.concatenate(sqs, axis=0)
        fade = fades[h]
        wr = betas[h] * (v - fade * pred)
        written[h] = wr
        read = fade * sq + kq * wr
        ho[:, h * hd : (h + 1) * hd] = (rms_scale(read, og[...]) * z).astype(BF16)

    wo_in.wait()
    mix[...] = jnp.dot(ho[...], wo[...], preferred_element_type=F32).astype(BF16)
    pl.semaphore_wait(barrier, 95 + shift)

    xchg = pltpu.make_async_remote_copy(
        mix, mix_in, sem_x.at[0], sem_x.at[1], device_id=partner, device_id_type=MESH
    )
    xchg.start()
    pushes = [
        pltpu.make_async_remote_copy(
            b.at[core], b.at[core], sem_push.at[i], sem_pull.at[i], device_id=partner, device_id_type=MESH
        )
        for i, b in enumerate((wg, wu, wdn))
    ]
    e_in[0].wait()
    pushes[0].start()
    tab_copy.wait()
    xchg.wait()

    resid = tok[...].astype(F32) + (mix[...].astype(F32) + mix_in[...].astype(F32))
    moe_in = rms_scale(resid, fgain[...])
    for t in range(tiles):
        moe32[pl.ds(t, seqs, stride=tiles), :] = moe_in[:, t * LANES : (t + 1) * LANES]

    @pl.when(core == 0)
    def _():
        res[...] = resid[:, :half]

    @pl.when(core == 1)
    def _():
        res[...] = resid[:, half:]

    for t in range(seqs):
        moe[t] = moe32[t * tiles : (t + 1) * tiles, :].astype(BF16)
    for d in range(n_ep):
        send[d] = moe[tab[core, d]]

    my_row = core * (n_ep // 2) + me // 2
    for a, b, c in order[:-1]:
        d = zs[a] + ys[b] + xs[c]
        pltpu.make_async_remote_copy(
            send.at[d], recv.at[my_row], sem_send, sem_recv, device_id={"ep": d, "tp": par}, device_id_type=MESH
        ).start()
    self_copy = pltpu.make_async_copy(send.at[me], recv.at[my_row], sem_recv)
    self_push = pltpu.make_async_remote_copy(
        send.at[me], recv.at[my_row], sem_self, sem_recv, device_id=partner, device_id_type=MESH
    )

    @pl.when(par == core)
    def _():
        self_copy.start()

    @pl.when(par != core)
    def _():
        self_push.start()

    for i in (1, 2):
        e_in[i].wait()
        pushes[i].start()

    for h in range(heads):
        for s in range(seqs):
            kcol = jnp.broadcast_to(kts[h, :, s : s + 1], (hd, hd))
            ns_ref[s, h] = fades[h, s : s + 1, :] * ns_ref[s, h] + kcol * written[h, s : s + 1, :]

    pltpu.make_async_copy(recv, recv, sem_recv).wait()
    for t in range(n_ep):
        rows32[t * tiles : (t + 1) * tiles, :] = recv[t].astype(F32)
    for t in range(tiles):
        lhs[:, t * LANES : (t + 1) * LANES] = rows32[pl.ds(t, n_ep, stride=tiles), :].astype(BF16)
    pushes[0].wait()
    pushes[1].wait()
    hid = []
    for p in range(2):
        g = jnp.dot(lhs[...], wg[p], preferred_element_type=F32)
        u = jnp.dot(lhs[...], wu[p], preferred_element_type=F32)
        hid.append((silu(g) * u).astype(BF16))
    pushes[2].wait()
    for t in range(tiles):
        cols = slice(t * LANES, (t + 1) * LANES)
        got = jnp.dot(hid[0], wdn[0, :, cols], preferred_element_type=F32) + jnp.dot(
            hid[1], wdn[1, :, cols], preferred_element_type=F32
        )
        term32[pl.ds(t, n_ep, stride=tiles), :] = got
    for i in range(n_ep // 2):
        for hh in range(2):
            for s in range(2):
                at = (s * (n_ep // 2) + i) * tiles + hh * htiles
                rsend[hh, i, s] = term32[at : at + htiles, :].astype(BF16)

    mine = pl.ds(2 * me, 2)
    for a, b, c in order[:-1]:
        if c % 2:
            continue
        d = zs[a] + ys[b] + xp[c]
        for hh in range(2):
            pltpu.make_async_remote_copy(
                rsend.at[hh, d // 2], ret.at[mine], sem_back, sem_home, device_id={"ep": d, "tp": hh}, device_id_type=MESH
            ).start()
    near = zs[0] + ys[0] + xp[0]
    back_other = pltpu.make_async_remote_copy(
        rsend.at[other, near // 2], ret.at[mine], sem_bself.at[0], sem_home,
        device_id={"ep": near, "tp": other}, device_id_type=MESH,
    )
    back_other.start()
    back_local = pltpu.make_async_copy(rsend.at[core, near // 2], ret.at[mine], sem_home)
    back_near = pltpu.make_async_remote_copy(
        rsend.at[core, near // 2], ret.at[mine], sem_bself.at[1], sem_home,
        device_id={"ep": near, "tp": core}, device_id_type=MESH,
    )

    @pl.when(par == core)
    def _():
        back_local.start()

    @pl.when(par != core)
    def _():
        back_near.start()

    pltpu.make_async_copy(send.at[pl.ds(0, n_ep - 1)], send.at[pl.ds(0, n_ep - 1)], sem_send).wait()

    @pl.when(par != core)
    def _():
        self_push.wait_send()

    pltpu.make_async_copy(
        rsend.at[:, pl.ds(0, n_ep // 2 - 1)], rsend.at[:, pl.ds(0, n_ep // 2 - 1)], sem_back
    ).wait()
    back_other.wait_send()

    @pl.when(par != core)
    def _():
        back_near.wait_send()

    pltpu.make_async_copy(ret, ret, sem_home).wait()
    for t in range(2 * n_ep):
        ret32[t] = ret[t].astype(F32)
    for t in range(seqs):
        acc = None
        for j in range(2):
            one = ret32[tab[2 + j, t]] * rw[j, t]
            acc = one if acc is None else acc + one
        acc32[t * htiles : (t + 1) * htiles, :] = acc
    for t in range(htiles):
        cols = slice(t * LANES, (t + 1) * LANES)
        out_ref[:, cols] = (res[:, cols] + acc32[pl.ds(t, seqs, stride=htiles), :]).astype(BF16)


def write_kernel(out_v, ns_v, out_h, ns_h, sem):
    parts = 4
    step = ns_v.shape[0] // parts
    copies = [pltpu.make_async_copy(out_v, out_h, sem.at[parts])] + [
        pltpu.make_async_copy(ns_v.at[pl.ds(i * step, step)], ns_h.at[pl.ds(i * step, step)], sem.at[i])
        for i in range(parts)
    ]
    for c in copies:
        c.start()
    for c in copies:
        c.wait()


HBM = pl.BlockSpec(memory_space=pltpu.HBM)
VMEM = pl.BlockSpec(memory_space=pltpu.VMEM)


def keep(a):
    return pltpu.with_memory_space_constraint(a, pltpu.HBM)


def per_device(
    dims,
    tokens, attn_gain, w_query, w_key, w_value, w_zgate, w_decay, w_beta, decay_rate, decay_bias,
    state, out_gain, w_out, ffn_gain, expert_gate, expert_up, expert_down, routes, route_weight,
):
    seqs, width = tokens.shape
    heads, hd = state.shape[1], state.shape[2]
    n_ep = lax.axis_size("ep")
    tiles = width // LANES
    hidden = expert_gate.shape[2]
    dma = pltpu.SemaphoreType.DMA
    smem, vmem = pltpu.SMEM, pltpu.VMEM

    args = (
        tokens, attn_gain.reshape(1, width), w_query, w_key, w_value, w_zgate, w_decay.T, w_beta.T, decay_rate,
        decay_bias, state, out_gain.reshape(1, hd), w_out, ffn_gain.reshape(1, width), expert_gate[0], expert_up[0],
        expert_down[0], routes.T, route_weight.T,
    )
    layer_out, new_state = pl.pallas_call(
        functools.partial(layer_kernel, n_ep, dims),
        name="layer",
        out_shape=(vmem((seqs, width // 2), BF16), vmem(state.shape, F32)),
        in_specs=[HBM] * len(args),
        out_specs=(VMEM, VMEM),
        scratch_shapes=[
            vmem((seqs, width), BF16),
            vmem((1, width), F32),
            vmem((heads, width, 4 * hd), BF16),
            vmem((heads, width), BF16),
            vmem((heads, width), BF16),
            smem((heads,), F32),
            smem((heads,), F32),
            vmem((1, hd), F32),
            vmem(w_out.shape, BF16),
            vmem((1, width), F32),
            vmem((2, seqs), jnp.int32),
            smem((2, seqs), F32),
            vmem((8, LANES), jnp.int32),
            smem((8, LANES), jnp.int32),
            vmem((heads, hd, seqs), F32),
            vmem((heads, seqs, hd), F32),
            vmem((heads, seqs, hd), F32),
            vmem((seqs, heads * hd), BF16),
            vmem((2, width, hidden), BF16),
            vmem((2, width, hidden), BF16),
            vmem((2, hidden, width), BF16),
            vmem((seqs, width), BF16),
            vmem((seqs, width), BF16),
            vmem((seqs * tiles, LANES), F32),
            vmem((seqs, tiles, LANES), BF16),
            vmem((n_ep, tiles, LANES), BF16),
            vmem((n_ep, tiles, LANES), BF16),
            vmem((n_ep * tiles, LANES), F32),
            vmem((n_ep, width), BF16),
            vmem((n_ep * tiles, LANES), F32),
            vmem((2, n_ep // 2, 2, tiles // 2, LANES), BF16),
            vmem((2 * n_ep, tiles // 2, LANES), BF16),
            vmem((2 * n_ep, tiles // 2, LANES), F32),
            vmem((seqs * tiles // 2, LANES), F32),
            vmem((seqs, width // 2), F32),
            dma((10,)), dma((heads, 4)), dma((heads,)), dma, dma, dma((3,)), dma((2,)), dma((3,)), dma((3,)),
            dma, dma, dma, dma, dma, dma((2,)),
        ],
        compiler_params=pltpu.CompilerParams(
            collective_id=0, has_side_effects=True, vmem_limit_bytes=40 * 2**20
        ),
    )(*[keep(a) for a in args])
    return pl.pallas_call(
        write_kernel,
        name="write",
        out_shape=(jax.ShapeDtypeStruct(layer_out.shape, BF16), jax.ShapeDtypeStruct(state.shape, F32)),
        in_specs=[VMEM, VMEM],
        out_specs=(HBM, HBM),
        scratch_shapes=[dma((5,))],
        compiler_params=pltpu.CompilerParams(vmem_limit_bytes=2**20),
    )(*[pltpu.with_memory_space_constraint(a, pltpu.VMEM) for a in (layer_out, new_state)])


def solution(mesh):
    in_specs = (
        P("ep", None), P(), P(None, "tp"), P(None, "tp"), P(None, "tp"), P(None, "tp"), P(None, "tp"), P(None, "tp"),
        P("tp"), P("tp"), P("ep", "tp", None, None), P(), P("tp", None), P(), P("ep", None, "tp"), P("ep", None, "tp"),
        P("ep", "tp", None), P("ep", None), P("ep", None),
    )
    out_specs = (P("ep", "tp"), P("ep", "tp", None, None))
    side = round(mesh.shape["ep"] ** (1 / 3))
    dims = (side, side, side)
    return jax.shard_map(
        functools.partial(per_device, dims), mesh=mesh, in_specs=in_specs, out_specs=out_specs, check_vma=False
    )
```

time: 55.8 us -> 32.9 us (0.59)
  local copies, waits for them, and re-layouts: 15.5 us -> 0 us
  Pallas kernels: 39.1 us -> 32.1 us
    unnamed x39 -> x0, local copies, waits for them, and re-layouts: 15.5 us -> none
    pallas_call x2, Pallas kernels: 39.1 us -> 32.1 us  [the longest x1 29.3 us: per_device(): pl.pallas_call(functools.partial(layer_kernel, n_ep, dims), name='layer',...]
where the time goes in v3:
time: 32.9 us; the launch traced here: 32.8 us
  Pallas kernels  32.1 us (98%)
  between operations  0.65 us (2%)
    pallas_call x1, Pallas kernels, per_device(): pl.pallas_call(functools.partial(layer_kernel, n_ep, dims), name='layer',...  29.3 us
    pallas_call x1, Pallas kernels, per_device(): pl.pallas_call(write_kernel, name='write', out_shape=(jax.ShapeDtypeStruc...  2.76 us

profile of v3, /device:TPU:1, one launch (start us, length us, event | category | flops | bytes accessed | tf_op | source)
XLA Modules:
  0.0 32.8 jit_solution(1001328834803089321)
XLA Ops:
  0.6 29.3 %layer.1 = (bf16[24,1024]{1,0:T(8,128)(2,1)S(1)}, f32[24,4,128,128]{3,2,1,0:T(8,128)S(1)}) custom-call(bf16[24,2048]{1,0:T(8,128)(2,1)} %tok_h.1, f32[1,2048]{1,0:T(1,128)} %bitcast.15, bf16[2048,512]{1,0:T(8,128)(2,1)} %wq_h.1, bf16[2048,512]{1,0:T(8,128)(2,1)} %wk_h.1, bf16[2048,512]{1,0:T(8,128)(2,1)} %wv_h.1, bf16[2048,512]{1,0:T(8,128)(2,1)} %wz_h.1, ...), custom_call_target="tpu_custom_call" | custom-call | tf_op jit(solution)/shard_map/layer/pallas_call | solution.py:377
  30.0 2.8 %write.1 = (bf16[24,1024]{1,0:T(8,128)(2,1)}, f32[24,4,128,128]{3,2,1,0:T(8,128)}) custom-call(bf16[24,1024]{1,0:T(8,128)(2,1)S(1)} %get-tuple-element.4.out_v, f32[24,4,128,128]{3,2,1,0:T(8,128)S(1)} %get-tuple-element.5.ns_v), custom_call_target="tpu_custom_call" | custom-call | tf_op jit(solution)/shard_map/write/pallas_call | solution.py:426

commit v4 on v3

--- a/solution.py
+++ b/solution.py
@@ -110,10 +110,10 @@
 
     pl.semaphore_signal(barrier, inc=1, device_id=partner, device_id_type=MESH)
 
+    for c in big[1]:
+        c.start()
     for c in small:
         c.wait()
-    for c in big[1]:
-        c.start()
 
     ids = lax.broadcasted_iota(jnp.int32, (n_ep, seqs), 0)
     row = lax.broadcasted_iota(jnp.int32, (n_ep, seqs), 1)
@@ -150,7 +150,7 @@
 
     sub = lax.broadcasted_iota(jnp.int32, (8, hd), 0)
     for h in range(heads):
-        for c in big[h]:
+        for c in big[h][:4]:
             c.wait()
         if h + 2 < heads:
             for c in big[h + 2]:
@@ -167,6 +167,7 @@
         z = silu(raw[:, 3 * hd : 4 * hd])
         kq = jnp.sum(k * q, axis=1, keepdims=True)
         kts[h] = k.T
+        big[h][4].wait()
         preds, sqs = [], []
         for g in range(seqs // 8):
             pair = jnp.concatenate([k[g * 8 : g * 8 + 8], q[g * 8 : g * 8 + 8]], axis=0).astype(BF16)
@@ -221,27 +222,34 @@
 
     for t in range(seqs):
         moe[t] = moe32[t * tiles : (t + 1) * tiles, :].astype(BF16)
-    for d in range(n_ep):
-        send[d] = moe[tab[core, d]]
-
-    my_row = core * (n_ep // 2) + me // 2
-    for a, b, c in order[:-1]:
-        d = zs[a] + ys[b] + xs[c]
+    targets = [(a, b, c) for a, b, c in order if c % 2 == 0]
+    dest = [zs[a] + ys[b] + xp[c] for a, b, c in targets]
+    count = len(dest)
+    pair = lambda i: pl.ds(2 * i, 2)
+    for i in range(count):
+        for slot in range(2):
+            send[2 * i + slot] = moe[tab[slot, dest[i]]]
+    group = z0 // (nz // 2)
+    landing = recv.at[pair(me // 2)]
+    for i in range(count - 1):
         pltpu.make_async_remote_copy(
-            send.at[d], recv.at[my_row], sem_send, sem_recv, device_id={"ep": d, "tp": par}, device_id_type=MESH
+            send.at[pair(i)], landing, sem_send, sem_recv.at[group],
+            device_id={"ep": dest[i], "tp": par}, device_id_type=MESH,
         ).start()
-    self_copy = pltpu.make_async_copy(send.at[me], recv.at[my_row], sem_recv)
-    self_push = pltpu.make_async_remote_copy(
-        send.at[me], recv.at[my_row], sem_self, sem_recv, device_id=partner, device_id_type=MESH
-    )
+    end = count - 1
+    end_far = pltpu.make_async_remote_copy(
+        send.at[pair(end)], landing, sem_self, sem_recv.at[group],
+        device_id={"ep": dest[end], "tp": par}, device_id_type=MESH,
+    )
+    end_local = pltpu.make_async_copy(send.at[pair(end)], landing, sem_recv.at[group])
+
+    @pl.when(par != core)
+    def _():
+        end_far.start()
 
     @pl.when(par == core)
     def _():
-        self_copy.start()
-
-    @pl.when(par != core)
-    def _():
-        self_push.start()
+        end_local.start()
 
     for i in (1, 2):
         e_in[i].wait()
@@ -252,74 +260,83 @@
             kcol = jnp.broadcast_to(kts[h, :, s : s + 1], (hd, hd))
             ns_ref[s, h] = fades[h, s : s + 1, :] * ns_ref[s, h] + kcol * written[h, s : s + 1, :]
 
-    pltpu.make_async_copy(recv, recv, sem_recv).wait()
-    for t in range(n_ep):
-        rows32[t * tiles : (t + 1) * tiles, :] = recv[t].astype(F32)
-    for t in range(tiles):
-        lhs[:, t * LANES : (t + 1) * LANES] = rows32[pl.ds(t, n_ep, stride=tiles), :].astype(BF16)
-    pushes[0].wait()
-    pushes[1].wait()
-    hid = []
-    for p in range(2):
-        g = jnp.dot(lhs[...], wg[p], preferred_element_type=F32)
-        u = jnp.dot(lhs[...], wu[p], preferred_element_type=F32)
-        hid.append((silu(g) * u).astype(BF16))
-    pushes[2].wait()
-    for t in range(tiles):
-        cols = slice(t * LANES, (t + 1) * LANES)
-        got = jnp.dot(hid[0], wdn[0, :, cols], preferred_element_type=F32) + jnp.dot(
-            hid[1], wdn[1, :, cols], preferred_element_type=F32
-        )
-        term32[pl.ds(t, n_ep, stride=tiles), :] = got
-    for i in range(n_ep // 2):
-        for hh in range(2):
-            for s in range(2):
-                at = (s * (n_ep // 2) + i) * tiles + hh * htiles
-                rsend[hh, i, s] = term32[at : at + htiles, :].astype(BF16)
-
-    mine = pl.ds(2 * me, 2)
-    for a, b, c in order[:-1]:
-        if c % 2:
-            continue
-        d = zs[a] + ys[b] + xp[c]
-        for hh in range(2):
-            pltpu.make_async_remote_copy(
-                rsend.at[hh, d // 2], ret.at[mine], sem_back, sem_home, device_id={"ep": d, "tp": hh}, device_id_type=MESH
-            ).start()
-    near = zs[0] + ys[0] + xp[0]
-    back_other = pltpu.make_async_remote_copy(
-        rsend.at[other, near // 2], ret.at[mine], sem_bself.at[0], sem_home,
-        device_id={"ep": near, "tp": other}, device_id_type=MESH,
-    )
-    back_other.start()
-    back_local = pltpu.make_async_copy(rsend.at[core, near // 2], ret.at[mine], sem_home)
-    back_near = pltpu.make_async_remote_copy(
-        rsend.at[core, near // 2], ret.at[mine], sem_bself.at[1], sem_home,
-        device_id={"ep": near, "tp": core}, device_id_type=MESH,
-    )
-
-    @pl.when(par == core)
-    def _():
-        back_local.start()
+    place = pl.ds(2 * me, 2)
+    rows = n_ep // 2
+    flat = sorted([(b, c) for b in range(ny) for c in range(0, nx, 2)], key=lambda o: -(hop(o[0], ny) + hop(o[1], nx)))
+    locals_ = []
+    for g in range(2):
+        here = recv.at[pl.ds(rows * g, rows)]
+        pltpu.make_async_copy(here, here, sem_recv.at[g]).wait()
+        for t in range(rows):
+            rows32[t * tiles : (t + 1) * tiles, :] = recv[rows * g + t].astype(F32)
+        for t in range(tiles):
+            lhs[:, t * LANES : (t + 1) * LANES] = rows32[pl.ds(t, rows, stride=tiles), :].astype(BF16)
+        if g == 0:
+            pushes[0].wait()
+            pushes[1].wait()
+        hid = []
+        for p in range(2):
+            gate = jnp.dot(lhs[...], wg[p], preferred_element_type=F32)
+            up = jnp.dot(lhs[...], wu[p], preferred_element_type=F32)
+            hid.append((silu(gate) * up).astype(BF16))
+        if g == 0:
+            pushes[2].wait()
+        for t in range(tiles):
+            cols = slice(t * LANES, (t + 1) * LANES)
+            got = jnp.dot(hid[0], wdn[0, :, cols], preferred_element_type=F32) + jnp.dot(
+                hid[1], wdn[1, :, cols], preferred_element_type=F32
+            )
+            term32[pl.ds(t, rows, stride=tiles), :] = got
+        for i in range(rows // 2):
+            for hh in range(2):
+                for slot in range(2):
+                    at = (2 * i + slot) * tiles + hh * htiles
+                    rsend[hh, g * (rows // 2) + i, slot] = term32[at : at + htiles, :].astype(BF16)
+
+        for b, c in flat:
+            for z in range(g * nz // 2, (g + 1) * nz // 2):
+                d = z * (ny * nx) + ys[b] + xp[c]
+                if b or c:
+                    for hh in range(2):
+                        pltpu.make_async_remote_copy(
+                            rsend.at[hh, d // 2], ret.at[place], sem_back, sem_home,
+                            device_id={"ep": d, "tp": hh}, device_id_type=MESH,
+                        ).start()
+                else:
+                    pltpu.make_async_remote_copy(
+                        rsend.at[other, d // 2], ret.at[place], sem_back, sem_home,
+                        device_id={"ep": d, "tp": other}, device_id_type=MESH,
+                    ).start()
+                    stays = (z == z0) & (par == core)
+                    back_far = pltpu.make_async_remote_copy(
+                        rsend.at[core, d // 2], ret.at[place], sem_bself.at[z], sem_home,
+                        device_id={"ep": d, "tp": core}, device_id_type=MESH,
+                    )
+                    back_local = pltpu.make_async_copy(rsend.at[core, d // 2], ret.at[place], sem_home)
+                    locals_.append((stays, back_far))
+
+                    @pl.when(stays)
+                    def _():
+                        back_local.start()
+
+                    @pl.when(jnp.logical_not(stays))
+                    def _():
+                        back_far.start()
+
+    sent = send.at[pl.ds(0, 2 * count - 2)]
+    pltpu.make_async_copy(sent, sent, sem_send).wait()
 
     @pl.when(par != core)
     def _():
-        back_near.start()
-
-    pltpu.make_async_copy(send.at[pl.ds(0, n_ep - 1)], send.at[pl.ds(0, n_ep - 1)], sem_send).wait()
-
-    @pl.when(par != core)
-    def _():
-        self_push.wait_send()
-
-    pltpu.make_async_copy(
-        rsend.at[:, pl.ds(0, n_ep // 2 - 1)], rsend.at[:, pl.ds(0, n_ep // 2 - 1)], sem_back
-    ).wait()
-    back_other.wait_send()
-
-    @pl.when(par != core)
-    def _():
-        back_near.wait_send()
+        end_far.wait_send()
+
+    sent = rsend.at[:, pl.ds(0, count - nz // 2)]
+    pltpu.make_async_copy(sent, sent, sem_back).wait()
+    for stays, back_far in locals_:
+
+        @pl.when(jnp.logical_not(stays))
+        def _():
+            back_far.wait_send()
 
     pltpu.make_async_copy(ret, ret, sem_home).wait()
     for t in range(2 * n_ep):
@@ -408,16 +425,16 @@
             vmem((seqs, tiles, LANES), BF16),
             vmem((n_ep, tiles, LANES), BF16),
             vmem((n_ep, tiles, LANES), BF16),
-            vmem((n_ep * tiles, LANES), F32),
-            vmem((n_ep, width), BF16),
-            vmem((n_ep * tiles, LANES), F32),
+            vmem((n_ep // 2 * tiles, LANES), F32),
+            vmem((n_ep // 2, width), BF16),
+            vmem((n_ep // 2 * tiles, LANES), F32),
             vmem((2, n_ep // 2, 2, tiles // 2, LANES), BF16),
             vmem((2 * n_ep, tiles // 2, LANES), BF16),
             vmem((2 * n_ep, tiles // 2, LANES), F32),
             vmem((seqs * tiles // 2, LANES), F32),
             vmem((seqs, width // 2), F32),
             dma((10,)), dma((heads, 4)), dma((heads,)), dma, dma, dma((3,)), dma((2,)), dma((3,)), dma((3,)),
-            dma, dma, dma, dma, dma, dma((2,)),
+            dma, dma((2,)), dma, dma, dma, dma((dims[0],)),
         ],
         compiler_params=pltpu.CompilerParams(
             collective_id=0, has_side_effects=True, vmem_limit_bytes=40 * 2**20

time: 32.9 us -> 30.4 us (0.924)
  Pallas kernels: 32.1 us -> 29.7 us
    pallas_call x1, Pallas kernels: 29.3 us -> 26.9 us  [per_device(): pl.pallas_call(functools.partial(layer_kernel, n_ep, dims), name='layer',...]
where the time goes in v4:
time: 30.4 us; the launch traced here: 30.3 us
  Pallas kernels  29.7 us (98%)
  between operations  0.65 us (2%)
    pallas_call x1, Pallas kernels, per_device(): pl.pallas_call(functools.partial(layer_kernel, n_ep, dims), name='layer',...  26.9 us
    pallas_call x1, Pallas kernels, per_device(): pl.pallas_call(write_kernel, name='write', out_shape=(jax.ShapeDtypeStruc...  2.76 us

profile of v4, /device:TPU:1, one launch (start us, length us, event | category | flops | bytes accessed | tf_op | source)
XLA Modules:
  0.0 30.3 jit_solution(3411312162044959796)
XLA Ops:
  0.6 26.9 %layer.1 = (bf16[24,1024]{1,0:T(8,128)(2,1)S(1)}, f32[24,4,128,128]{3,2,1,0:T(8,128)S(1)}) custom-call(bf16[24,2048]{1,0:T(8,128)(2,1)} %tok_h.1, f32[1,2048]{1,0:T(1,128)} %bitcast.15, bf16[2048,512]{1,0:T(8,128)(2,1)} %wq_h.1, bf16[2048,512]{1,0:T(8,128)(2,1)} %wk_h.1, bf16[2048,512]{1,0:T(8,128)(2,1)} %wv_h.1, bf16[2048,512]{1,0:T(8,128)(2,1)} %wz_h.1, ...), custom_call_target="tpu_custom_call" | custom-call | tf_op jit(solution)/shard_map/layer/pallas_call | solution.py:394
  27.6 2.8 %write.1 = (bf16[24,1024]{1,0:T(8,128)(2,1)}, f32[24,4,128,128]{3,2,1,0:T(8,128)}) custom-call(bf16[24,1024]{1,0:T(8,128)(2,1)S(1)} %get-tuple-element.4.out_v, f32[24,4,128,128]{3,2,1,0:T(8,128)S(1)} %get-tuple-element.5.ns_v), custom_call_target="tpu_custom_call" | custom-call | tf_op jit(solution)/shard_map/write/pallas_call | solution.py:443

commit v5 on v4

--- a/solution.py
+++ b/solution.py
@@ -30,12 +30,30 @@
     return jnp.maximum(x, 0.0) + jnp.log(1.0 + jnp.exp(-jnp.abs(x)))
 
 
+def split_plane(ny, nx):
+    hops = lambda o: min(o[0], ny - o[0]) + min(o[1], nx - o[1])
+    back = lambda o: (-o[0] % ny, -o[1] % nx)
+    every = [(b, c) for b in range(ny) for c in range(nx)]
+    every.sort(key=lambda o: (-hops(o), o == back(o), min(o, back(o))))
+    half = len(every) // 2
+    far, near = every[:half], every[half:]
+    if any(back(o) not in far for o in far):
+        odd = next(o for o in far if back(o) not in far)
+        own = next(o for o in near if o == back(o) and any(o))
+        far[far.index(odd)], near[near.index(own)] = own, odd
+    assert all(back(o) in far for o in far)
+    return far, near
+
+
+CUTS = (0, 1, 2, 4)
+
+
 def layer_kernel(
     n_ep, dims,
     tok_h, gain_h, wq_h, wk_h, wv_h, wz_h, wd_h, wb_h, rate_h, bias_h, st_h, og_h, wo_h, fgain_h, eg_h, eu_h, ed_h, rt_h, rw_h,
     out_ref, ns_ref,
     tok, gain, wbuf, wd, wb, rate, bias, og, wo, fgain, rt, rw, tab_v, tab,
-    kts, written, fades, ho,
+    kts, written, fades, ho, mix32,
     wg, wu, wdn, mix, mix_in, moe32, moe, send, recv, rows32, lhs, term32, rsend, ret, ret32, acc32, res,
     sem_small, sem_w, sem_s, sem_wo, sem_tab, sem_e, sem_x, sem_push, sem_pull, sem_send, sem_recv, sem_self, sem_back, sem_home, sem_bself,
 ):
@@ -47,8 +65,6 @@
     me = lax.axis_index("ep")
     core = lax.axis_index("tp")
     other = 1 - core
-    par = lax.rem(me, 2)
-    shift = jnp.where(par == core, 0, 1)
     nz, ny, nx = dims
 
     small = [
@@ -77,41 +93,60 @@
         pltpu.make_async_copy(a, b.at[core], sem_e.at[i])
         for i, (a, b) in enumerate([(eg_h, wg), (eu_h, wu), (ed_h, wdn)])
     ]
-    for c in big[0]:
-        c.start()
+    units = []
+    for h in range(heads):
+        units.append(big[h][:4])
+        if h + 1 == heads:
+            units.append([wo_in])
+        units.append(big[h][4:])
+    units += [e_in, [], [], []]
+    for u in units[:2]:
+        for c in u:
+            c.start()
+
+    def take(n):
+        for c in units[n]:
+            c.wait()
+        for c in units[n + 4]:
+            c.start()
 
     z0, y0, x0 = me // (ny * nx), lax.rem(me // nx, ny), lax.rem(me, nx)
     zs = [lax.rem(z0 + i, nz) * (ny * nx) for i in range(nz)]
     ys = [lax.rem(y0 + i, ny) * nx for i in range(ny)]
     xs = [lax.rem(x0 + i, nx) for i in range(nx)]
-    xp = [lax.rem(x0 + i + shift, nx) for i in range(nx)]
+    far, near = split_plane(ny, nx)
+    count = len(far)
+    ahead = lambda o: ys[o[0]] + xs[o[1]]
+    behind = lambda o: ys[-o[0] % ny] + xs[-o[1] % nx]
+    mine = [jnp.where(core == 1, ahead(f), ahead(n)) for f, n in zip(far, near)]
+    their = [jnp.where(core == 1, ahead(n), ahead(f)) for f, n in zip(far, near)]
+    home = [jnp.where(core == 1, behind(f), behind(n)) for f, n in zip(far, near)]
     hop = lambda i, n: min(i, n - i)
     order = sorted(
-        [(a, b, c) for a in range(nz) for b in range(ny) for c in range(nx)],
-        key=lambda o: -(hop(o[0], nz) + hop(o[1], ny) + hop(o[2], nx)),
-    )
+        [(a, j) for a in range(nz) for j in range(count)],
+        key=lambda o: (-(hop(o[0], nz) + hop(far[o[1]][0], ny) + hop(far[o[1]][1], nx)), -o[0]),
+    )
+    order.remove((0, count - 1))
+    order.append((0, count - 1))
     partner = {"ep": me, "tp": other}
 
     barrier = pltpu.get_barrier_semaphore()
-    for a, b, c in order[:-1]:
-        pl.semaphore_signal(
-            barrier, inc=1, device_id={"ep": zs[a] + ys[b] + xs[c], "tp": par}, device_id_type=MESH
-        )
-        if c % 2 == 0:
-            pl.semaphore_signal(
-                barrier, inc=1, device_id={"ep": zs[a] + ys[b] + xp[c], "tp": 1 - par}, device_id_type=MESH
-            )
-
-    @pl.when(par != core)
-    def _():
-        pl.semaphore_signal(
-            barrier, inc=1, device_id={"ep": zs[0] + ys[0] + xp[0], "tp": 1 - par}, device_id_type=MESH
-        )
-
-    pl.semaphore_signal(barrier, inc=1, device_id=partner, device_id_type=MESH)
-
-    for c in big[1]:
-        c.start()
+    for a, j in order[:-1]:
+        pl.semaphore_signal(barrier, inc=1, device_id={"ep": zs[a] + mine[j], "tp": core}, device_id_type=MESH)
+        pl.semaphore_signal(barrier, inc=1, device_id={"ep": zs[a] + mine[j], "tp": other}, device_id_type=MESH)
+        pl.semaphore_signal(barrier, inc=1, device_id={"ep": zs[a] + their[j], "tp": other}, device_id_type=MESH)
+    last = zs[0] + mine[count - 1]
+
+    @pl.when(core == 1)
+    def _():
+        pl.semaphore_signal(barrier, inc=1, device_id={"ep": last, "tp": core}, device_id_type=MESH)
+
+    pl.semaphore_signal(barrier, inc=1, device_id={"ep": last, "tp": other}, device_id_type=MESH)
+    pl.semaphore_signal(barrier, inc=1, device_id={"ep": zs[0] + their[count - 1], "tp": other}, device_id_type=MESH)
+
+    for u in units[2:4]:
+        for c in u:
+            c.start()
     for c in small:
         c.wait()
 
@@ -121,11 +156,11 @@
     hits = [ids == r[j : j + 1, :] for j in range(2)]
     either = hits[0] | hits[1]
     first = jnp.min(jnp.where(either, row, seqs), axis=1, keepdims=True)
-    last = jnp.max(jnp.where(either, row, 0), axis=1, keepdims=True)
+    final = jnp.max(jnp.where(either, row, 0), axis=1, keepdims=True)
     first_row = jnp.where(first == seqs, 0, first)
     diag = lax.broadcasted_iota(jnp.int32, (n_ep, n_ep), 0) == lax.broadcasted_iota(jnp.int32, (n_ep, n_ep), 1)
     tab_v[0:1, 0:n_ep] = jnp.sum(jnp.where(diag, first_row, 0), axis=0, keepdims=True)
-    tab_v[1:2, 0:n_ep] = jnp.sum(jnp.where(diag, last, 0), axis=0, keepdims=True)
+    tab_v[1:2, 0:n_ep] = jnp.sum(jnp.where(diag, final, 0), axis=0, keepdims=True)
     later = jnp.where(row > first, 1, 0)
     for j in range(2):
         slot = jnp.sum(jnp.where(hits[j], later, 0), axis=0, keepdims=True)
@@ -149,36 +184,28 @@
     tab_copy.start()
 
     sub = lax.broadcasted_iota(jnp.int32, (8, hd), 0)
-    for h in range(heads):
-        for c in big[h][:4]:
-            c.wait()
-        if h + 2 < heads:
-            for c in big[h + 2]:
-                c.start()
-        if h + 2 == heads:
-            wo_in.start()
-        if h + 1 == heads:
-            for c in e_in:
-                c.start()
-        raw = jnp.dot(normed, wbuf[h], preferred_element_type=F32).astype(BF16).astype(F32)
+
+    def project(h):
+        return jnp.dot(normed, wbuf[h], preferred_element_type=F32).astype(BF16).astype(F32)
+
+    def mixing(h, raw):
         q = unit_rows(silu(raw[:, 0:hd])) * hd ** (-0.5)
         k = unit_rows(silu(raw[:, hd : 2 * hd]))
         v = silu(raw[:, 2 * hd : 3 * hd])
         z = silu(raw[:, 3 * hd : 4 * hd])
         kq = jnp.sum(k * q, axis=1, keepdims=True)
         kts[h] = k.T
-        big[h][4].wait()
         preds, sqs = [], []
         for g in range(seqs // 8):
-            pair = jnp.concatenate([k[g * 8 : g * 8 + 8], q[g * 8 : g * 8 + 8]], axis=0).astype(BF16)
+            both = jnp.concatenate([k[g * 8 : g * 8 + 8], q[g * 8 : g * 8 + 8]], axis=0).astype(BF16)
             pred = sq = None
             for s in range(0, 8, 2):
-                both = jnp.concatenate([ns_ref[g * 8 + s, h], ns_ref[g * 8 + s + 1, h]], axis=1).astype(BF16)
-                got = jnp.dot(pair, both, preferred_element_type=F32)
+                two = jnp.concatenate([ns_ref[g * 8 + s, h], ns_ref[g * 8 + s + 1, h]], axis=1).astype(BF16)
+                got = jnp.dot(both, two, preferred_element_type=F32)
                 for i in range(2):
-                    one, two = got[0:8, i * hd : (i + 1) * hd], got[8:16, i * hd : (i + 1) * hd]
-                    pred = one if pred is None else jnp.where(sub == s + i, one, pred)
-                    sq = two if sq is None else jnp.where(sub == s + i, two, sq)
+                    top, low = got[0:8, i * hd : (i + 1) * hd], got[8:16, i * hd : (i + 1) * hd]
+                    pred = top if pred is None else jnp.where(sub == s + i, top, pred)
+                    sq = low if sq is None else jnp.where(sub == s + i, low, sq)
             preds.append(pred)
             sqs.append(sq)
         pred, sq = jnp.concatenate(preds, axis=0), jnp.concatenate(sqs, axis=0)
@@ -188,9 +215,21 @@
         read = fade * sq + kq * wr
         ho[:, h * hd : (h + 1) * hd] = (rms_scale(read, og[...]) * z).astype(BF16)
 
-    wo_in.wait()
-    mix[...] = jnp.dot(ho[...], wo[...], preferred_element_type=F32).astype(BF16)
-    pl.semaphore_wait(barrier, 95 + shift)
+    early = (heads - 1) * hd
+    take(0)
+    raw = project(0)
+    for h in range(heads - 1):
+        take(2 * h + 1)
+        take(2 * h + 2)
+        after = project(h + 1)
+        mixing(h, raw)
+        raw = after
+    take(2 * heads - 1)
+    mix32[...] = jnp.dot(ho[:, :early], wo[:early], preferred_element_type=F32)
+    take(2 * heads)
+    mixing(heads - 1, raw)
+    mix[...] = (mix32[...] + jnp.dot(ho[:, early:], wo[early:], preferred_element_type=F32)).astype(BF16)
+    pl.semaphore_wait(barrier, 3 * nz * count - 1 + core)
 
     xchg = pltpu.make_async_remote_copy(
         mix, mix_in, sem_x.at[0], sem_x.at[1], device_id=partner, device_id_type=MESH
@@ -222,32 +261,29 @@
 
     for t in range(seqs):
         moe[t] = moe32[t * tiles : (t + 1) * tiles, :].astype(BF16)
-    targets = [(a, b, c) for a, b, c in order if c % 2 == 0]
-    dest = [zs[a] + ys[b] + xp[c] for a, b, c in targets]
-    count = len(dest)
     pair = lambda i: pl.ds(2 * i, 2)
-    for i in range(count):
+    for i, (a, j) in enumerate(order):
         for slot in range(2):
-            send[2 * i + slot] = moe[tab[slot, dest[i]]]
-    group = z0 // (nz // 2)
-    landing = recv.at[pair(me // 2)]
-    for i in range(count - 1):
+            send[2 * i + slot] = moe[tab[slot, zs[a] + mine[j]]]
+    cuts = CUTS
+    group = sum(jnp.where(z0 >= cut, 1, 0) for cut in cuts[1:-1])
+    end = len(order) - 1
+    for i, (a, j) in enumerate(order[:-1]):
         pltpu.make_async_remote_copy(
-            send.at[pair(i)], landing, sem_send, sem_recv.at[group],
-            device_id={"ep": dest[i], "tp": par}, device_id_type=MESH,
+            send.at[pair(i)], recv.at[pair(z0 * count + j)], sem_send, sem_recv.at[group],
+            device_id={"ep": zs[a] + mine[j], "tp": core}, device_id_type=MESH,
         ).start()
-    end = count - 1
+    landing = recv.at[pair(z0 * count + count - 1)]
     end_far = pltpu.make_async_remote_copy(
-        send.at[pair(end)], landing, sem_self, sem_recv.at[group],
-        device_id={"ep": dest[end], "tp": par}, device_id_type=MESH,
+        send.at[pair(end)], landing, sem_self, sem_recv.at[group], device_id={"ep": last, "tp": core}, device_id_type=MESH
     )
     end_local = pltpu.make_async_copy(send.at[pair(end)], landing, sem_recv.at[group])
 
-    @pl.when(par != core)
+    @pl.when(core == 1)
     def _():
         end_far.start()
 
-    @pl.when(par == core)
+    @pl.when(core == 0)
     def _():
         end_local.start()
 
@@ -261,23 +297,23 @@
             ns_ref[s, h] = fades[h, s : s + 1, :] * ns_ref[s, h] + kcol * written[h, s : s + 1, :]
 
     place = pl.ds(2 * me, 2)
-    rows = n_ep // 2
-    flat = sorted([(b, c) for b in range(ny) for c in range(0, nx, 2)], key=lambda o: -(hop(o[0], ny) + hop(o[1], nx)))
+    per_z = 2 * count
     locals_ = []
-    for g in range(2):
-        here = recv.at[pl.ds(rows * g, rows)]
+    for g in range(len(cuts) - 1):
+        low, rows = cuts[g] * per_z, (cuts[g + 1] - cuts[g]) * per_z
+        here = recv.at[pl.ds(low, rows)]
         pltpu.make_async_copy(here, here, sem_recv.at[g]).wait()
         for t in range(rows):
-            rows32[t * tiles : (t + 1) * tiles, :] = recv[rows * g + t].astype(F32)
+            rows32[t * tiles : (t + 1) * tiles, :] = recv[low + t].astype(F32)
         for t in range(tiles):
-            lhs[:, t * LANES : (t + 1) * LANES] = rows32[pl.ds(t, rows, stride=tiles), :].astype(BF16)
+            lhs[:rows, t * LANES : (t + 1) * LANES] = rows32[pl.ds(t, rows, stride=tiles), :].astype(BF16)
         if g == 0:
             pushes[0].wait()
             pushes[1].wait()
         hid = []
         for p in range(2):
-            gate = jnp.dot(lhs[...], wg[p], preferred_element_type=F32)
-            up = jnp.dot(lhs[...], wu[p], preferred_element_type=F32)
+            gate = jnp.dot(lhs[:rows], wg[p], preferred_element_type=F32)
+            up = jnp.dot(lhs[:rows], wu[p], preferred_element_type=F32)
             hid.append((silu(gate) * up).astype(BF16))
         if g == 0:
             pushes[2].wait()
@@ -291,28 +327,24 @@
             for hh in range(2):
                 for slot in range(2):
                     at = (2 * i + slot) * tiles + hh * htiles
-                    rsend[hh, g * (rows // 2) + i, slot] = term32[at : at + htiles, :].astype(BF16)
-
-        for b, c in flat:
-            for z in range(g * nz // 2, (g + 1) * nz // 2):
-                d = z * (ny * nx) + ys[b] + xp[c]
-                if b or c:
-                    for hh in range(2):
+                    rsend[hh, low // 2 + i, slot] = term32[at : at + htiles, :].astype(BF16)
+
+        for j in range(count):
+            for z in range(cuts[g], cuts[g + 1]):
+                d, i = z * (ny * nx) + home[j], z * count + j
+                for hh in range(2):
+                    if hh == 1 or j + 1 < count:
                         pltpu.make_async_remote_copy(
-                            rsend.at[hh, d // 2], ret.at[place], sem_back, sem_home,
+                            rsend.at[hh, i], ret.at[place], sem_back, sem_home,
                             device_id={"ep": d, "tp": hh}, device_id_type=MESH,
                         ).start()
-                else:
-                    pltpu.make_async_remote_copy(
-                        rsend.at[other, d // 2], ret.at[place], sem_back, sem_home,
-                        device_id={"ep": d, "tp": other}, device_id_type=MESH,
-                    ).start()
-                    stays = (z == z0) & (par == core)
+                        continue
+                    stays = (z == z0) & (core == 0)
                     back_far = pltpu.make_async_remote_copy(
-                        rsend.at[core, d // 2], ret.at[place], sem_bself.at[z], sem_home,
-                        device_id={"ep": d, "tp": core}, device_id_type=MESH,
+                        rsend.at[hh, i], ret.at[place], sem_bself.at[z], sem_home,
+                        device_id={"ep": d, "tp": hh}, device_id_type=MESH,
                     )
-                    back_local = pltpu.make_async_copy(rsend.at[core, d // 2], ret.at[place], sem_home)
+                    back_local = pltpu.make_async_copy(rsend.at[hh, i], ret.at[place], sem_home)
                     locals_.append((stays, back_far))
 
                     @pl.when(stays)
@@ -323,14 +355,14 @@
                     def _():
                         back_far.start()
 
-    sent = send.at[pl.ds(0, 2 * count - 2)]
+    sent = send.at[pl.ds(0, 2 * end)]
     pltpu.make_async_copy(sent, sent, sem_send).wait()
 
-    @pl.when(par != core)
+    @pl.when(core == 1)
     def _():
         end_far.wait_send()
 
-    sent = rsend.at[:, pl.ds(0, count - nz // 2)]
+    sent = rsend.at[:, pl.ds(0, nz * count - nz // 2)]
     pltpu.make_async_copy(sent, sent, sem_back).wait()
     for stays, back_far in locals_:
 
@@ -416,6 +448,7 @@
             vmem((heads, seqs, hd), F32),
             vmem((heads, seqs, hd), F32),
             vmem((seqs, heads * hd), BF16),
+            vmem((seqs, width), F32),
             vmem((2, width, hidden), BF16),
             vmem((2, width, hidden), BF16),
             vmem((2, hidden, width), BF16),
@@ -434,7 +467,7 @@
             vmem((seqs * tiles // 2, LANES), F32),
             vmem((seqs, width // 2), F32),
             dma((10,)), dma((heads, 4)), dma((heads,)), dma, dma, dma((3,)), dma((2,)), dma((3,)), dma((3,)),
-            dma, dma((2,)), dma, dma, dma, dma((dims[0],)),
+            dma, dma((3,)), dma, dma, dma, dma((dims[0],)),
         ],
         compiler_params=pltpu.CompilerParams(
             collective_id=0, has_side_effects=True, vmem_limit_bytes=40 * 2**20

time: 30.4 us -> 28.9 us (0.951)
  Pallas kernels: 29.7 us -> 28.1 us
    pallas_call x1, Pallas kernels: 26.9 us -> 25.3 us  [per_device(): pl.pallas_call(functools.partial(layer_kernel, n_ep, dims), name='layer',...]
where the time goes in v5:
time: 28.9 us; the launch traced here: 28.8 us
  Pallas kernels  28.1 us (97%)
  between operations  0.65 us (2%)
    pallas_call x1, Pallas kernels, per_device(): pl.pallas_call(functools.partial(layer_kernel, n_ep, dims), name='layer',...  25.3 us
    pallas_call x1, Pallas kernels, per_device(): pl.pallas_call(write_kernel, name='write', out_shape=(jax.ShapeDtypeStruc...  2.76 us

profile of v5, /device:TPU:1, one launch (start us, length us, event | category | flops | bytes accessed | tf_op | source)
XLA Modules:
  0.0 28.8 jit_solution(1216864348796158727)
XLA Ops:
  0.6 25.3 %layer.1 = (bf16[24,1024]{1,0:T(8,128)(2,1)S(1)}, f32[24,4,128,128]{3,2,1,0:T(8,128)S(1)}) custom-call(bf16[24,2048]{1,0:T(8,128)(2,1)} %tok_h.1, f32[1,2048]{1,0:T(1,128)} %bitcast.15, bf16[2048,512]{1,0:T(8,128)(2,1)} %wq_h.1, bf16[2048,512]{1,0:T(8,128)(2,1)} %wk_h.1, bf16[2048,512]{1,0:T(8,128)(2,1)} %wv_h.1, bf16[2048,512]{1,0:T(8,128)(2,1)} %wz_h.1, ...), custom_call_target="tpu_custom_call" | custom-call | tf_op jit(solution)/shard_map/layer/pallas_call | solution.py:426
  26.0 2.8 %write.1 = (bf16[24,1024]{1,0:T(8,128)(2,1)}, f32[24,4,128,128]{3,2,1,0:T(8,128)}) custom-call(bf16[24,1024]{1,0:T(8,128)(2,1)S(1)} %get-tuple-element.4.out_v, f32[24,4,128,128]{3,2,1,0:T(8,128)S(1)} %get-tuple-element.5.ns_v), custom_call_target="tpu_custom_call" | custom-call | tf_op jit(solution)/shard_map/write/pallas_call | solution.py:476

commit v6 on v5

--- a/solution.py
+++ b/solution.py
@@ -55,7 +55,7 @@
     tok, gain, wbuf, wd, wb, rate, bias, og, wo, fgain, rt, rw, tab_v, tab,
     kts, written, fades, ho, mix32,
     wg, wu, wdn, mix, mix_in, moe32, moe, send, recv, rows32, lhs, term32, rsend, ret, ret32, acc32, res,
-    sem_small, sem_w, sem_s, sem_wo, sem_tab, sem_e, sem_x, sem_push, sem_pull, sem_send, sem_recv, sem_self, sem_back, sem_home, sem_bself,
+    sem_small, sem_w, sem_s, sem_wo, sem_x, sem_pull, sem_recv, sem_home,
 ):
     seqs, width = tok.shape
     heads, hd = kts.shape[0], kts.shape[1]
@@ -83,30 +83,32 @@
         cols = pl.ds(h * hd, hd)
         big.append(
             [
-                pltpu.make_async_copy(w.at[:, cols], wbuf.at[h, :, pl.ds(i * hd, hd)], sem_w.at[h, i])
+                pltpu.make_async_copy(w.at[:, cols], wbuf.at[h, :, pl.ds(i * hd, hd)], sem_w.at[h])
                 for i, w in enumerate((wq_h, wk_h, wv_h, wz_h))
             ]
             + [pltpu.make_async_copy(st_h.at[:, h], ns_ref.at[:, h], sem_s.at[h])]
         )
     wo_in = pltpu.make_async_copy(wo_h, wo, sem_wo)
     e_in = [
-        pltpu.make_async_copy(a, b.at[core], sem_e.at[i])
+        pltpu.make_async_copy(a, b.at[core], sem_small.at[1 + i])
         for i, (a, b) in enumerate([(eg_h, wg), (eu_h, wu), (ed_h, wdn)])
     ]
-    units = []
+    units, waits = [], []
     for h in range(heads):
         units.append(big[h][:4])
+        waits.append(pltpu.make_async_copy(wbuf.at[h], wbuf.at[h], sem_w.at[h]))
         if h + 1 == heads:
             units.append([wo_in])
+            waits.append(wo_in)
         units.append(big[h][4:])
+        waits.append(big[h][4])
     units += [e_in, [], [], []]
     for u in units[:2]:
         for c in u:
             c.start()
 
     def take(n):
-        for c in units[n]:
-            c.wait()
+        waits[n].wait()
         for c in units[n + 4]:
             c.start()
 
@@ -124,7 +126,7 @@
     hop = lambda i, n: min(i, n - i)
     order = sorted(
         [(a, j) for a in range(nz) for j in range(count)],
-        key=lambda o: (-(hop(o[0], nz) + hop(far[o[1]][0], ny) + hop(far[o[1]][1], nx)), -o[0]),
+        key=lambda o: (-(hop(o[0], nz) + hop(far[o[1]][0], ny) + hop(far[o[1]][1], nx)), o[1] % 3, -o[0]),
     )
     order.remove((0, count - 1))
     order.append((0, count - 1))
@@ -180,7 +182,7 @@
         fades[h] = jnp.broadcast_to(fade, (seqs, hd))
         betas.append(jnp.broadcast_to(1.0 / (1.0 + jnp.exp(-narrow(wb, h))), (seqs, hd)))
 
-    tab_copy = pltpu.make_async_copy(tab_v, tab, sem_tab)
+    tab_copy = pltpu.make_async_copy(tab_v, tab, sem_small.at[0])
     tab_copy.start()
 
     sub = lax.broadcasted_iota(jnp.int32, (8, hd), 0)
@@ -188,13 +190,16 @@
     def project(h):
         return jnp.dot(normed, wbuf[h], preferred_element_type=F32).astype(BF16).astype(F32)
 
-    def mixing(h, raw):
+    def gates(h, raw):
         q = unit_rows(silu(raw[:, 0:hd])) * hd ** (-0.5)
         k = unit_rows(silu(raw[:, hd : 2 * hd]))
         v = silu(raw[:, 2 * hd : 3 * hd])
         z = silu(raw[:, 3 * hd : 4 * hd])
         kq = jnp.sum(k * q, axis=1, keepdims=True)
         kts[h] = k.T
+        return q, k, v, z, kq
+
+    def mixing(h, q, k, v, z, kq):
         preds, sqs = [], []
         for g in range(seqs // 8):
             both = jnp.concatenate([k[g * 8 : g * 8 + 8], q[g * 8 : g * 8 + 8]], axis=0).astype(BF16)
@@ -222,22 +227,23 @@
         take(2 * h + 1)
         take(2 * h + 2)
         after = project(h + 1)
-        mixing(h, raw)
+        mixing(h, *gates(h, raw))
         raw = after
     take(2 * heads - 1)
+    ready = gates(heads - 1, raw)
     mix32[...] = jnp.dot(ho[:, :early], wo[:early], preferred_element_type=F32)
     take(2 * heads)
-    mixing(heads - 1, raw)
+    mixing(heads - 1, *ready)
     mix[...] = (mix32[...] + jnp.dot(ho[:, early:], wo[early:], preferred_element_type=F32)).astype(BF16)
     pl.semaphore_wait(barrier, 3 * nz * count - 1 + core)
 
     xchg = pltpu.make_async_remote_copy(
-        mix, mix_in, sem_x.at[0], sem_x.at[1], device_id=partner, device_id_type=MESH
+        mix, mix_in, sem_small.at[4], sem_x, device_id=partner, device_id_type=MESH
     )
     xchg.start()
     pushes = [
         pltpu.make_async_remote_copy(
-            b.at[core], b.at[core], sem_push.at[i], sem_pull.at[i], device_id=partner, device_id_type=MESH
+            b.at[core], b.at[core], sem_small.at[5 + i], sem_pull.at[i], device_id=partner, device_id_type=MESH
         )
         for i, b in enumerate((wg, wu, wdn))
     ]
@@ -266,6 +272,7 @@
         for slot in range(2):
             send[2 * i + slot] = moe[tab[slot, zs[a] + mine[j]]]
     cuts = CUTS
+    sem_send, sem_self, sem_back = sem_small.at[8], sem_small.at[9], sem_wo
     group = sum(jnp.where(z0 >= cut, 1, 0) for cut in cuts[1:-1])
     end = len(order) - 1
     for i, (a, j) in enumerate(order[:-1]):
@@ -317,22 +324,20 @@
             hid.append((silu(gate) * up).astype(BF16))
         if g == 0:
             pushes[2].wait()
-        for t in range(tiles):
-            cols = slice(t * LANES, (t + 1) * LANES)
-            got = jnp.dot(hid[0], wdn[0, :, cols], preferred_element_type=F32) + jnp.dot(
-                hid[1], wdn[1, :, cols], preferred_element_type=F32
-            )
-            term32[pl.ds(t, rows, stride=tiles), :] = got
-        for i in range(rows // 2):
-            for hh in range(2):
+        for hh in range(2):
+            for t in range(hh * htiles, (hh + 1) * htiles):
+                cols = slice(t * LANES, (t + 1) * LANES)
+                got = jnp.dot(hid[0], wdn[0, :, cols], preferred_element_type=F32) + jnp.dot(
+                    hid[1], wdn[1, :, cols], preferred_element_type=F32
+                )
+                term32[pl.ds(t, rows, stride=tiles), :] = got
+            for i in range(rows // 2):
                 for slot in range(2):
                     at = (2 * i + slot) * tiles + hh * htiles
                     rsend[hh, low // 2 + i, slot] = term32[at : at + htiles, :].astype(BF16)
-
-        for j in range(count):
-            for z in range(cuts[g], cuts[g + 1]):
-                d, i = z * (ny * nx) + home[j], z * count + j
-                for hh in range(2):
+            for j in range(count):
+                for z in range(cuts[g], cuts[g + 1]):
+                    d, i = z * (ny * nx) + home[j], z * count + j
                     if hh == 1 or j + 1 < count:
                         pltpu.make_async_remote_copy(
                             rsend.at[hh, i], ret.at[place], sem_back, sem_home,
@@ -341,7 +346,7 @@
                         continue
                     stays = (z == z0) & (core == 0)
                     back_far = pltpu.make_async_remote_copy(
-                        rsend.at[hh, i], ret.at[place], sem_bself.at[z], sem_home,
+                        rsend.at[hh, i], ret.at[place], sem_w.at[z], sem_home,
                         device_id={"ep": d, "tp": hh}, device_id_type=MESH,
                     )
                     back_local = pltpu.make_async_copy(rsend.at[hh, i], ret.at[place], sem_home)
@@ -466,8 +471,7 @@
             vmem((2 * n_ep, tiles // 2, LANES), F32),
             vmem((seqs * tiles // 2, LANES), F32),
             vmem((seqs, width // 2), F32),
-            dma((10,)), dma((heads, 4)), dma((heads,)), dma, dma, dma((3,)), dma((2,)), dma((3,)), dma((3,)),
-            dma, dma((3,)), dma, dma, dma, dma((dims[0],)),
+            dma((10,)), dma((heads,)), dma((heads,)), dma, dma, dma((3,)), dma((len(CUTS) - 1,)), dma,
         ],
         compiler_params=pltpu.CompilerParams(
             collective_id=0, has_side_effects=True, vmem_limit_bytes=40 * 2**20

time: 28.9 us -> 28.4 us (0.983)
  Pallas kernels: 28.1 us -> 27.7 us
    pallas_call x1, Pallas kernels: 25.3 us -> 24.9 us  [per_device(): pl.pallas_call(functools.partial(layer_kernel, n_ep, dims), name='layer',...]
where the time goes in v6:
time: 28.4 us; the launch traced here: 28.3 us
  Pallas kernels  27.7 us (98%)
  between operations  0.65 us (2%)
    pallas_call x1, Pallas kernels, per_device(): pl.pallas_call(functools.partial(layer_kernel, n_ep, dims), name='layer',...  24.9 us
    pallas_call x1, Pallas kernels, per_device(): pl.pallas_call(write_kernel, name='write', out_shape=(jax.ShapeDtypeStruc...  2.76 us

profile of v6, /device:TPU:1, one launch (start us, length us, event | category | flops | bytes accessed | tf_op | source)
XLA Modules:
  0.0 28.3 jit_solution(5262661810593333849)
XLA Ops:
  0.6 24.9 %layer.1 = (bf16[24,1024]{1,0:T(8,128)(2,1)S(1)}, f32[24,4,128,128]{3,2,1,0:T(8,128)S(1)}) custom-call(bf16[24,2048]{1,0:T(8,128)(2,1)} %tok_h.1, f32[1,2048]{1,0:T(1,128)} %bitcast.15, bf16[2048,512]{1,0:T(8,128)(2,1)} %wq_h.1, bf16[2048,512]{1,0:T(8,128)(2,1)} %wk_h.1, bf16[2048,512]{1,0:T(8,128)(2,1)} %wv_h.1, bf16[2048,512]{1,0:T(8,128)(2,1)} %wz_h.1, ...), custom_call_target="tpu_custom_call" | custom-call | tf_op jit(solution)/shard_map/layer/pallas_call | solution.py:431
  25.6 2.8 %write.1 = (bf16[24,1024]{1,0:T(8,128)(2,1)}, f32[24,4,128,128]{3,2,1,0:T(8,128)}) custom-call(bf16[24,1024]{1,0:T(8,128)(2,1)S(1)} %get-tuple-element.4.out_v, f32[24,4,128,128]{3,2,1,0:T(8,128)S(1)} %get-tuple-element.5.ns_v), custom_call_target="tpu_custom_call" | custom-call | tf_op jit(solution)/shard_map/write/pallas_call | solution.py:480

commit v7 on v6

--- a/solution.py
+++ b/solution.py
@@ -53,7 +53,7 @@
     tok_h, gain_h, wq_h, wk_h, wv_h, wz_h, wd_h, wb_h, rate_h, bias_h, st_h, og_h, wo_h, fgain_h, eg_h, eu_h, ed_h, rt_h, rw_h,
     out_ref, ns_ref,
     tok, gain, wbuf, wd, wb, rate, bias, og, wo, fgain, rt, rw, tab_v, tab,
-    kts, written, fades, ho, mix32,
+    kts, written, fades, ho, mix32, raw32,
     wg, wu, wdn, mix, mix_in, moe32, moe, send, recv, rows32, lhs, term32, rsend, ret, ret32, acc32, res,
     sem_small, sem_w, sem_s, sem_wo, sem_x, sem_pull, sem_recv, sem_home,
 ):
@@ -78,30 +78,27 @@
     ]
     for c in small:
         c.start()
-    big = []
-    for h in range(heads):
-        cols = pl.ds(h * hd, hd)
-        big.append(
-            [
-                pltpu.make_async_copy(w.at[:, cols], wbuf.at[h, :, pl.ds(i * hd, hd)], sem_w.at[h])
-                for i, w in enumerate((wq_h, wk_h, wv_h, wz_h))
-            ]
-            + [pltpu.make_async_copy(st_h.at[:, h], ns_ref.at[:, h], sem_s.at[h])]
-        )
+    chunks = 4
+    depth = width // chunks
+    part = lambda c: pl.ds(c * depth, depth)
+    s_in = [pltpu.make_async_copy(st_h.at[:, h], ns_ref.at[:, h], sem_s.at[h]) for h in range(heads)]
     wo_in = pltpu.make_async_copy(wo_h, wo, sem_wo)
     e_in = [
         pltpu.make_async_copy(a, b.at[core], sem_small.at[1 + i])
         for i, (a, b) in enumerate([(eg_h, wg), (eu_h, wu), (ed_h, wdn)])
     ]
     units, waits = [], []
-    for h in range(heads):
-        units.append(big[h][:4])
-        waits.append(pltpu.make_async_copy(wbuf.at[h], wbuf.at[h], sem_w.at[h]))
-        if h + 1 == heads:
-            units.append([wo_in])
-            waits.append(wo_in)
-        units.append(big[h][4:])
-        waits.append(big[h][4])
+    for c in range(chunks):
+        units.append(
+            [
+                pltpu.make_async_copy(w.at[part(c)], wbuf.at[i, part(c)], sem_w.at[c])
+                for i, w in enumerate((wq_h, wk_h, wv_h, wz_h))
+            ]
+        )
+        waits.append(pltpu.make_async_copy(wbuf.at[:, part(c)], wbuf.at[:, part(c)], sem_w.at[c]))
+    for c in s_in[:-1] + [wo_in] + s_in[-1:]:
+        units.append([c])
+        waits.append(c)
     units += [e_in, [], [], []]
     for u in units[:2]:
         for c in u:
@@ -187,14 +184,12 @@
 
     sub = lax.broadcasted_iota(jnp.int32, (8, hd), 0)
 
-    def project(h):
-        return jnp.dot(normed, wbuf[h], preferred_element_type=F32).astype(BF16).astype(F32)
-
     def gates(h, raw):
-        q = unit_rows(silu(raw[:, 0:hd])) * hd ** (-0.5)
-        k = unit_rows(silu(raw[:, hd : 2 * hd]))
-        v = silu(raw[:, 2 * hd : 3 * hd])
-        z = silu(raw[:, 3 * hd : 4 * hd])
+        bits = [r[:, h * hd : (h + 1) * hd].astype(BF16).astype(F32) for r in raw]
+        q = unit_rows(silu(bits[0])) * hd ** (-0.5)
+        k = unit_rows(silu(bits[1]))
+        v = silu(bits[2])
+        z = silu(bits[3])
         kq = jnp.sum(k * q, axis=1, keepdims=True)
         kts[h] = k.T
         return q, k, v, z, kq
@@ -221,19 +216,22 @@
         ho[:, h * hd : (h + 1) * hd] = (rms_scale(read, og[...]) * z).astype(BF16)
 
     early = (heads - 1) * hd
-    take(0)
-    raw = project(0)
+    for c in range(chunks):
+        take(c)
+        for i in range(4):
+            rows = slice(c * depth, (c + 1) * depth)
+            got = jnp.dot(normed[:, rows], wbuf[i, rows], preferred_element_type=F32)
+            raw32[i] = got if c == 0 else raw32[i] + got
+    raw = [raw32[i] for i in range(4)]
     for h in range(heads - 1):
-        take(2 * h + 1)
-        take(2 * h + 2)
-        after = project(h + 1)
-        mixing(h, *gates(h, raw))
-        raw = after
-    take(2 * heads - 1)
+        ready = gates(h, raw)
+        take(chunks + h)
+        mixing(h, *ready)
     ready = gates(heads - 1, raw)
+    take(chunks + heads - 1)
+    take(chunks + heads)
+    mixing(heads - 1, *ready)
     mix32[...] = jnp.dot(ho[:, :early], wo[:early], preferred_element_type=F32)
-    take(2 * heads)
-    mixing(heads - 1, *ready)
     mix[...] = (mix32[...] + jnp.dot(ho[:, early:], wo[early:], preferred_element_type=F32)).astype(BF16)
     pl.semaphore_wait(barrier, 3 * nz * count - 1 + core)
 
@@ -437,7 +435,7 @@
         scratch_shapes=[
             vmem((seqs, width), BF16),
             vmem((1, width), F32),
-            vmem((heads, width, 4 * hd), BF16),
+            vmem((4, width, heads * hd), BF16),
             vmem((heads, width), BF16),
             vmem((heads, width), BF16),
             smem((heads,), F32),
@@ -454,6 +452,7 @@
             vmem((heads, seqs, hd), F32),
             vmem((seqs, heads * hd), BF16),
             vmem((seqs, width), F32),
+            vmem((4, seqs, heads * hd), F32),
             vmem((2, width, hidden), BF16),
             vmem((2, width, hidden), BF16),
             vmem((2, hidden, width), BF16),

time: 28.4 us -> 28.4 us (level)
  no operation moved by 1% of the time
where the time goes in v7:
time: 28.4 us; the launch traced here: 28.3 us
  Pallas kernels  27.6 us (97%)
  between operations  0.65 us (2%)
    pallas_call x1, Pallas kernels, per_device(): pl.pallas_call(functools.partial(layer_kernel, n_ep, dims), name='layer',...  24.8 us
    pallas_call x1, Pallas kernels, per_device(): pl.pallas_call(write_kernel, name='write', out_shape=(jax.ShapeDtypeStruc...  2.76 us

profile of v7, /device:TPU:1, one launch (start us, length us, event | category | flops | bytes accessed | tf_op | source)
XLA Modules:
  0.0 28.3 jit_solution(12771478451072226364)
XLA Ops:
  0.6 24.8 %layer.1 = (bf16[24,1024]{1,0:T(8,128)(2,1)S(1)}, f32[24,4,128,128]{3,2,1,0:T(8,128)S(1)}) custom-call(bf16[24,2048]{1,0:T(8,128)(2,1)} %tok_h.1, f32[1,2048]{1,0:T(1,128)} %bitcast.15, bf16[2048,512]{1,0:T(8,128)(2,1)} %wq_h.1, bf16[2048,512]{1,0:T(8,128)(2,1)} %wk_h.1, bf16[2048,512]{1,0:T(8,128)(2,1)} %wv_h.1, bf16[2048,512]{1,0:T(8,128)(2,1)} %wz_h.1, ...), custom_call_target="tpu_custom_call" | custom-call | tf_op jit(solution)/shard_map/layer/pallas_call | solution.py:429
  25.5 2.8 %write.1 = (bf16[24,1024]{1,0:T(8,128)(2,1)}, f32[24,4,128,128]{3,2,1,0:T(8,128)}) custom-call(bf16[24,1024]{1,0:T(8,128)(2,1)S(1)} %get-tuple-element.4.out_v, f32[24,4,128,128]{3,2,1,0:T(8,128)S(1)} %get-tuple-element.5.ns_v), custom_call_target="tpu_custom_call" | custom-call | tf_op jit(solution)/shard_map/write/pallas_call | solution.py:479

commit v8 on v7

--- a/solution.py
+++ b/solution.py
@@ -99,7 +99,7 @@
     for c in s_in[:-1] + [wo_in] + s_in[-1:]:
         units.append([c])
         waits.append(c)
-    units += [e_in, [], [], []]
+    units += [[], e_in, [], []]
     for u in units[:2]:
         for c in u:
             c.start()
@@ -229,9 +229,9 @@
         mixing(h, *ready)
     ready = gates(heads - 1, raw)
     take(chunks + heads - 1)
+    mix32[...] = jnp.dot(ho[:, :early], wo[:early], preferred_element_type=F32)
     take(chunks + heads)
     mixing(heads - 1, *ready)
-    mix32[...] = jnp.dot(ho[:, :early], wo[:early], preferred_element_type=F32)
     mix[...] = (mix32[...] + jnp.dot(ho[:, early:], wo[early:], preferred_element_type=F32)).astype(BF16)
     pl.semaphore_wait(barrier, 3 * nz * count - 1 + core)
 

time: 28.4 us -> 28.3 us (level)
  no operation moved by 1% of the time
where the time goes in v8:
time: 28.3 us; the launch traced here: 28.2 us
  Pallas kernels  27.6 us (98%)
  between operations  0.65 us (2%)
    pallas_call x1, Pallas kernels, per_device(): pl.pallas_call(functools.partial(layer_kernel, n_ep, dims), name='layer',...  24.8 us
    pallas_call x1, Pallas kernels, per_device(): pl.pallas_call(write_kernel, name='write', out_shape=(jax.ShapeDtypeStruc...  2.76 us

profile of v8, /device:TPU:1, one launch (start us, length us, event | category | flops | bytes accessed | tf_op | source)
XLA Modules:
  0.0 28.2 jit_solution(7349287471475708723)
XLA Ops:
  0.6 24.8 %layer.1 = (bf16[24,1024]{1,0:T(8,128)(2,1)S(1)}, f32[24,4,128,128]{3,2,1,0:T(8,128)S(1)}) custom-call(bf16[24,2048]{1,0:T(8,128)(2,1)} %tok_h.1, f32[1,2048]{1,0:T(1,128)} %bitcast.15, bf16[2048,512]{1,0:T(8,128)(2,1)} %wq_h.1, bf16[2048,512]{1,0:T(8,128)(2,1)} %wk_h.1, bf16[2048,512]{1,0:T(8,128)(2,1)} %wv_h.1, bf16[2048,512]{1,0:T(8,128)(2,1)} %wz_h.1, ...), custom_call_target="tpu_custom_call" | custom-call | tf_op jit(solution)/shard_map/layer/pallas_call | solution.py:429
  25.5 2.8 %write.1 = (bf16[24,1024]{1,0:T(8,128)(2,1)}, f32[24,4,128,128]{3,2,1,0:T(8,128)}) custom-call(bf16[24,1024]{1,0:T(8,128)(2,1)S(1)} %get-tuple-element.4.out_v, f32[24,4,128,128]{3,2,1,0:T(8,128)S(1)} %get-tuple-element.5.ns_v), custom_call_target="tpu_custom_call" | custom-call | tf_op jit(solution)/shard_map/write/pallas_call | solution.py:479
